TPU v7x, 256 devices: a whole 4x4x8 slice. The times are simulated.
256 devices in a mesh: tp: 32 (over z, x), dp: 8 (over y, core).
Axes of the slice: x: 4, y: 4, z: 8, core: 2. Of those that a mesh axis runs over, the one named last changes fastest.
Arguments:
- tokens: bfloat16 [256, 8, 4096], P('dp', None, 'tp'), may hold values from -12 to 12
- lengths: int32 [256], P('dp'), may hold values from 1 to 8, 768 in all
- norm_gains: float32 [2, 4096], replicated, may hold values from 0.1 to 1.9
- drive_proj: bfloat16 [2, 4096, 2048], P(None, 'dp', 'tp'), may hold values from -0.09375 to 0.09375
- open_proj: bfloat16 [2, 4096, 4096], P(None, 'dp', 'tp'), may hold values from -0.09375 to 0.09375
- glu_proj: bfloat16 [2, 2048, 2048], P(None, 'dp', 'tp'), may hold values from -0.125 to 0.125
- merge_proj: bfloat16 [2, 2048, 4096], P(None, 'dp', 'tp'), may hold values from -0.125 to 0.125
- exit_proj: bfloat16 [2, 4096, 4096], P(None, 'dp', 'tp'), may hold values from -0.09375 to 0.09375
- decay_rate: float32 [2, 128, 64], P(None, 'tp'), may hold values from 0.5 to 2
- turn_rate: float32 [2, 128, 64], P(None, 'tp'), may hold values from -3 to 3
- group_step_width: float32 [2, 128], P(None, 'tp'), may hold values from 0.005 to 0.3
- state_in: float32 [2, 2, 128, 64, 16], P(None, None, 'tp'), may hold values from -1 to 1
- state_out: float32 [2, 2, 128, 16, 64], P(None, None, 'tp'), may hold values from -0.5 to 0.5
- skip_gain: float32 [2, 2048], P(None, 'tp'), may hold values from -4 to 4
- carried_state: float32 [2, 2, 256, 8192], P(None, None, 'dp', 'tp'), may hold values from -6 to 6
Outputs:
- updated_tokens: bfloat16 [256, 8, 4096], P('dp', None, 'tp')
- new_state: float32 [2, 2, 256, 8192], P(None, None, 'dp', 'tp')
Inputs may be any that keep to these rules, and one draw needn't show every extreme that they name: `lengths`: each sequence has at least one live slot, and some sequence has all 8.
All inputs are finite; a program needn't handle non-finite values. No bound on the sum of `lengths` on one device may be relied on, other than what follows from the above.
Results may differ from a plain program's by a relative error of at most 0.0055.
Values may be sent and summed in bfloat16 or wider, within the bound.
A program may use at most 64 MiB of HBM per device.

v0:
```python
import jax
import jax.numpy as jnp
from jax import lax
from jax.sharding import Mesh
from jax.sharding import PartitionSpec as P

TP = ("tp_0", "tp_1")


EPS = 1e-05


def gathered_by_axis(array, axes, dim):
    if not axes:
        return array
    nearer = lax.all_gather(array, axes[-1], axis=dim, tiled=True)
    return gathered_by_axis(nearer, axes[:-1], dim)


def copy_for_each(array, axis):
    size = lax.axis_size(axis)
    return lax.all_to_all(
        jnp.broadcast_to(array[None], (size, *array.shape)), axis, 0, 0, tiled=True
    )


def joined_along(parts, dim):
    parts = jnp.moveaxis(parts, 0, dim)
    dims = parts.shape
    return parts.reshape(*dims[:dim], dims[dim] * dims[dim + 1], *dims[dim + 2 :])


def gather_directly(array, axis, dim):
    parts = copy_for_each(array, axis)
    return joined_along(parts, dim)


def state_update(
    drive, active, current_rate, turn_now, size_now, in_pair, output_couple, skip_now, carried
):
    sequences, positions = active.shape
    groups, entries = current_rate.shape
    members = in_pair.shape[-1]
    real_eig = -current_rate
    step_len = size_now[:, None]
    magnitude = jnp.exp(step_len * real_eig)
    decay_real = magnitude * jnp.cos(step_len * turn_now)
    decay_imag = magnitude * jnp.sin(step_len * turn_now)
    divisor = real_eig * real_eig + turn_now * turn_now
    hold_real = ((decay_real - 1.0) * real_eig + decay_imag * turn_now) / divisor
    hold_imag = (decay_imag * real_eig - (decay_real - 1.0) * turn_now) / divisor
    inject_real = hold_real[..., None] * in_pair[0] - hold_imag[..., None] * in_pair[1]
    inject_imag = hold_real[..., None] * in_pair[1] + hold_imag[..., None] * in_pair[0]
    inputs = drive.reshape(sequences, positions, groups, members)
    pushed_real = jnp.einsum("gpc,bsgc->bsgp", inject_real, inputs)
    pushed_imag = jnp.einsum("gpc,bsgc->bsgp", inject_imag, inputs)
    state_real_part = carried[0].reshape(sequences, groups, entries)
    state_imaginary = carried[1].reshape(sequences, groups, entries)
    readings = []
    for position in range(positions):
        active_now = (active[:, position] > 0)[:, None, None]
        moved_real = (
            decay_real * state_real_part - decay_imag * state_imaginary + pushed_real[:, position]
        )
        moved_imag = (
            decay_real * state_imaginary + decay_imag * state_real_part + pushed_imag[:, position]
        )
        state_real_part = jnp.where(active_now, moved_real, state_real_part)
        state_imaginary = jnp.where(active_now, moved_imag, state_imaginary)
        readout_value = jnp.einsum("sal,usl->usa", output_couple[0], state_real_part) - jnp.einsum(
            "sal,usl->usa", output_couple[1], state_imaginary
        )
        readings.append(readout_value)
    readout = jnp.stack(readings, axis=1) + skip_now.reshape(groups, members) * inputs
    final = jnp.stack(
        [
            state_real_part.reshape(sequences, groups * entries),
            state_imaginary.reshape(sequences, groups * entries),
        ]
    )
    return (readout.reshape(sequences * positions, groups * members), final)


def widen_model(values):
    return gathered_by_axis(values, TP, 1)


def widen_branch(values):
    return gather_directly(values, TP, 1)


def project(gathered, weight):
    return jnp.dot(gathered, gather_directly(weight, "dp", 0), preferred_element_type=jnp.float32)


def shards(
    tokens,
    lengths,
    norm_gains,
    drive_proj,
    open_proj,
    glu_proj,
    merge_proj,
    exit_proj,
    decay_rate,
    turn_rate,
    group_step_width,
    state_in,
    state_out,
    skip_gain,
    carried_state,
):
    sequences, positions, local_width = tokens.shape
    row_count = sequences * positions
    active = (lax.broadcasted_iota(jnp.int32, (sequences, positions), 1) < lengths[:, None]).astype(
        jnp.int32
    )
    active_rows = active.reshape(row_count, 1).astype(jnp.float32)
    residual = tokens.reshape(row_count, local_width)
    states = []
    for layer_index in range(norm_gains.shape[0]):
        norm_gain = norm_gains[layer_index]
        whole = widen_model(residual).astype(jnp.float32)
        inverse_rms = lax.rsqrt(jnp.mean(whole * whole, axis=1, keepdims=True) + EPS)
        gathered = (whole * inverse_rms * norm_gain).astype(jnp.bfloat16)
        drive = project(gathered, drive_proj[layer_index])
        gate_open = jax.nn.sigmoid(project(gathered, open_proj[layer_index]))
        readout, final = state_update(
            drive,
            active,
            decay_rate[layer_index],
            turn_rate[layer_index],
            group_step_width[layer_index],
            state_in[layer_index],
            state_out[layer_index],
            skip_gain[layer_index],
            carried_state[layer_index],
        )
        states.append(final)
        activated = jax.nn.gelu(readout).astype(jnp.bfloat16)
        gating = project(widen_branch(activated), glu_proj[layer_index])
        gated = (activated.astype(jnp.float32) * jax.nn.sigmoid(gating)).astype(jnp.bfloat16)
        merged = project(widen_branch(gated), merge_proj[layer_index])
        mixed = (gate_open * merged).astype(jnp.bfloat16)
        branch = project(widen_model(mixed), exit_proj[layer_index])
        residual = (residual.astype(jnp.float32) + active_rows * branch).astype(jnp.bfloat16)
    return (residual.reshape(sequences, positions, local_width), jnp.stack(states))


def solution(mesh):
    split = Mesh(mesh.devices.reshape(8, 4, mesh.shape["dp"]), ("tp_0", "tp_1", "dp"))
    placed = (
        P("dp", None, TP),
        P("dp"),
        P(),
        P(None, "dp", TP),
        P(None, "dp", TP),
        P(None, "dp", TP),
        P(None, "dp", TP),
        P(None, "dp", TP),
        P(None, TP, None),
        P(None, TP, None),
        P(None, TP),
        P(None, None, TP, None, None),
        P(None, None, TP, None, None),
        P(None, TP),
        P(None, None, "dp", TP),
    )
    return jax.shard_map(
        shards,
        mesh=split,
        in_specs=placed,
        out_specs=(P("dp", None, TP), P(None, None, "dp", TP)),
        check_vma=False,
    )
```

profile of v0, /device:TPU:32, one launch (start us, length us, event | category | flops | bytes accessed | tf_op | source)
XLA Modules:
  0.0 454.8 jit_solution(13153953348340885512)
XLA Ops:
  7.3 13.0 %all_gather.24 = bf16[256,512]{1,0:T(8,128)(2,1)} all-gather(bf16[256,128]{1,0:T(8,128)(2,1)} %bitcast.849), channel_id=1, replica_groups=mesh['tp_0'=8,'tp_1'=4,'dp'=8] {'tp_1'}, dimensions={1}, use_global_device_ids=true | all-gather | bytes 327680 | tf_op jit(solution)/shard_map/all_gather | solution.py:16
  22.1 4.5 all-to-all-start.1
  29.6 7.2 %all-to-all-done.1 = bf16[8,512,64]{1,2,0:T(8,128)(2,1)S(1)} async-done(((bf16[8,512,64]{1,2,0:T(8,128)(2,1)}), bf16[8,512,64]{1,2,0:T(8,128)(2,1)S(1)}, u32[]{:S(2)}, u32[]{:S(2)}) %all-to-all-start.1) | async-done | bytes 524320 | tf_op jit(solution)/shard_map/all_to_all | solution.py:22
  37.6 3.4 all-to-all-start.3
  41.0 22.8 %all-gather.5.cloned.1.call-done = bf16[256,4096]{1,0:T(8,128)(2,1)} async-done(((bf16[256,512]{1,0:T(8,128)(2,1)}), bf16[256,4096]{1,0:T(8,128)(2,1)}) %all-gather.5.cloned.1.call-update) | async-done | bytes 2097168 | tf_op jit(solution)/shard_map/all_gather | solution.py:16
  63.8 2.2 fusion
  66.1 1.3 fusion.8
  72.2 1.1 broadcast_in_dim.328
  73.3 7.6 %all-to-all-start.2 = ((bf16[32,256,64]{1,2,0:T(8,128)(2,1)}), bf16[32,256,64]{1,2,0:T(8,128)(2,1)S(1)}, u32[]{:S(2)}, u32[]{:S(2)}) async-start(bf16[32,256,64]{1,2,0:T(8,128)(2,1)} %broadcast_in_dim.328), calls=%async_computation.2 | async-start | bytes 2097152 | tf_op jit(solution)/shard_map/all_to_all | solution.py:22
  81.6 22.5 %all-to-all-done.2 = bf16[32,256,64]{1,2,0:T(8,128)(2,1)S(1)} async-done(((bf16[32,256,64]{1,2,0:T(8,128)(2,1)}), bf16[32,256,64]{1,2,0:T(8,128)(2,1)S(1)}, u32[]{:S(2)}, u32[]{:S(2)}) %all-to-all-start.2) | async-done | bytes 1048608 | tf_op jit(solution)/shard_map/all_to_all | solution.py:22
  104.9 4.3 all-to-all-start.5
  109.5 10.0 %all-to-all-done.5 = bf16[8,256,128]{2,1,0:T(8,128)(2,1)S(1)} async-done(((bf16[8,256,128]{2,1,0:T(8,128)(2,1)}), bf16[8,256,128]{2,1,0:T(8,128)(2,1)S(1)}, u32[]{:S(2)}, u32[]{:S(2)}) %all-to-all-start.5) | async-done | bytes 524320 | tf_op jit(solution)/shard_map/all_to_all | solution.py:22
  120.6 6.1 %all-to-all-start.4 = ((bf16[32,256,64]{1,2,0:T(8,128)(2,1)}), bf16[32,256,64]{1,2,0:T(8,128)(2,1)S(1)}, u32[]{:S(2)}, u32[]{:S(2)}) async-start(bf16[32,256,64]{1,2,0:T(8,128)(2,1)} %broadcast_in_dim.331), calls=%async_computation.4 | async-start | bytes 2097152 | tf_op jit(solution)/shard_map/all_to_all | solution.py:22
  127.4 26.2 %all-to-all-done.4 = bf16[32,256,64]{1,2,0:T(8,128)(2,1)S(1)} async-done(((bf16[32,256,64]{1,2,0:T(8,128)(2,1)}), bf16[32,256,64]{1,2,0:T(8,128)(2,1)S(1)}, u32[]{:S(2)}, u32[]{:S(2)}) %all-to-all-start.4) | async-done | bytes 1048608 | tf_op jit(solution)/shard_map/all_to_all | solution.py:22
  153.6 1.1 broadcast_in_dim.317
  154.7 4.4 all-to-all-start
  159.6 15.4 %all-to-all-done = bf16[8,512,128]{2,1,0:T(8,128)(2,1)} async-done(((bf16[8,512,128]{2,1,0:T(8,128)(2,1)}), bf16[8,512,128]{2,1,0:T(8,128)(2,1)}, u32[]{:S(2)}, u32[]{:S(2)}) %all-to-all-start) | async-done | bytes 1048608 | tf_op jit(solution)/shard_map/all_to_all | solution.py:22
  175.0 2.7 fusion.23
  177.7 12.7 %all_gather.26 = bf16[256,512]{1,0:T(8,128)(2,1)} all-gather(bf16[256,128]{1,0:T(8,128)(2,1)S(1)} %fusion.23), channel_id=1, replica_groups=mesh['tp_0'=8,'tp_1'=4,'dp'=8] {'tp_1'}, dimensions={1}, use_global_device_ids=true | all-gather | bytes 327680 | tf_op jit(solution)/shard_map/all_gather | solution.py:16
  191.1 1.1 broadcast_in_dim.335
  192.2 3.6 all-to-all-start.6
  196.0 15.6 %all-to-all-done.6 = bf16[8,512,128]{2,1,0:T(8,128)(2,1)S(1)} async-done(((bf16[8,512,128]{2,1,0:T(8,128)(2,1)}), bf16[8,512,128]{2,1,0:T(8,128)(2,1)S(1)}, u32[]{:S(2)}, u32[]{:S(2)}) %all-to-all-start.6) | async-done | bytes 1048608 | tf_op jit(solution)/shard_map/all_to_all | solution.py:22
  211.6 15.7 %all-gather.7.cloned.1.call-done = bf16[256,4096]{1,0:T(8,128)(2,1)} async-done(((bf16[256,512]{1,0:T(8,128)(2,1)}), bf16[256,4096]{1,0:T(8,128)(2,1)}) %all-gather.7.cloned.1.call-update) | async-done | bytes 2097168 | tf_op jit(solution)/shard_map/all_gather | solution.py:16
  227.3 2.3 fusion.20
  230.3 12.7 %all_gather.28 = bf16[256,512]{1,0:T(8,128)(2,1)} all-gather(bf16[256,128]{1,0:T(8,128)(2,1)S(1)} %fusion.20), channel_id=1, replica_groups=mesh['tp_0'=8,'tp_1'=4,'dp'=8] {'tp_1'}, dimensions={1}, use_global_device_ids=true | all-gather | bytes 327680 | tf_op jit(solution)/shard_map/all_gather | solution.py:16
  243.8 4.3 all-to-all-start.8
  248.9 9.4 %all-to-all-done.8 = bf16[8,512,64]{1,2,0:T(8,128)(2,1)S(1)} async-done(((bf16[8,512,64]{1,2,0:T(8,128)(2,1)}), bf16[8,512,64]{1,2,0:T(8,128)(2,1)S(1)}, u32[]{:S(2)}, u32[]{:S(2)}) %all-to-all-start.8) | async-done | bytes 524320 | tf_op jit(solution)/shard_map/all_to_all | solution.py:22
  259.1 3.6 all-to-all-start.10
  262.8 18.8 %all-gather.9.cloned.1.call-done = bf16[256,4096]{1,0:T(8,128)(2,1)} async-done(((bf16[256,512]{1,0:T(8,128)(2,1)}), bf16[256,4096]{1,0:T(8,128)(2,1)}) %all-gather.9.cloned.1.call-update) | async-done | bytes 2097168 | tf_op jit(solution)/shard_map/all_gather | solution.py:16
  281.6 2.2 fusion.3
  284.4 1.3 fusion.6
  291.9 30.5 %all_to_all.70 = bf16[32,256,64]{1,2,0:T(8,128)(2,1)S(1)} all-to-all(bf16[32,256,64]{1,2,0:T(8,128)(2,1)S(1)} %broadcast_in_dim.340), channel_id=1, replica_groups=mesh['tp_0'=8,'tp_1'=4,'dp'=8] {'tp_0','tp_1'}, dimensions={0} | all-to-all | bytes 2097152 | tf_op jit(solution)/shard_map/all_to_all | solution.py:22
  322.4 1.7 broadcast_in_dim.345
  324.1 4.3 all-to-all-start.12
  328.4 1.1 fusion.33
  329.5 9.3 %all-to-all-done.12 = bf16[8,256,128]{2,1,0:T(8,128)(2,1)} async-done(((bf16[8,256,128]{2,1,0:T(8,128)(2,1)}), bf16[8,256,128]{2,1,0:T(8,128)(2,1)}, u32[]{:S(2)}, u32[]{:S(2)}) %all-to-all-start.12) | async-done | bytes 524320 | tf_op jit(solution)/shard_map/all_to_all | solution.py:22
  338.9 32.8 %all_to_all.71 = bf16[32,256,64]{1,2,0:T(8,128)(2,1)S(1)} all-to-all(bf16[32,256,64]{1,2,0:T(8,128)(2,1)S(1)} %broadcast_in_dim.343), channel_id=1, replica_groups=mesh['tp_0'=8,'tp_1'=4,'dp'=8] {'tp_0','tp_1'}, dimensions={0} | all-to-all | bytes 2097152 | tf_op jit(solution)/shard_map/all_to_all | solution.py:22
  371.7 1.1 broadcast_in_dim.337
  372.8 4.4 all-to-all-start.7
  377.2 1.5 fusion.312
  378.7 14.4 %all-to-all-done.7 = bf16[8,512,128]{2,1,0:T(8,128)(2,1)} async-done(((bf16[8,512,128]{2,1,0:T(8,128)(2,1)}), bf16[8,512,128]{2,1,0:T(8,128)(2,1)}, u32[]{:S(2)}, u32[]{:S(2)}) %all-to-all-start.7) | async-done | bytes 1048608 | tf_op jit(solution)/shard_map/all_to_all | solution.py:22
  393.1 2.7 fusion.22
  395.8 12.7 %all_gather.30 = bf16[256,512]{1,0:T(8,128)(2,1)} all-gather(bf16[256,128]{1,0:T(8,128)(2,1)S(1)} %fusion.22), channel_id=1, replica_groups=mesh['tp_0'=8,'tp_1'=4,'dp'=8] {'tp_1'}, dimensions={1}, use_global_device_ids=true | all-gather | bytes 327680 | tf_op jit(solution)/shard_map/all_gather | solution.py:16
  408.5 1.1 broadcast_in_dim.347
  409.7 3.6 all-to-all-start.13
  424.5 4.6 %all-to-all-done.13 = bf16[8,512,128]{2,1,0:T(8,128)(2,1)S(1)} async-done(((bf16[8,512,128]{2,1,0:T(8,128)(2,1)}), bf16[8,512,128]{2,1,0:T(8,128)(2,1)S(1)}, u32[]{:S(2)}, u32[]{:S(2)}) %all-to-all-start.13) | async-done | bytes 1048608 | tf_op jit(solution)/shard_map/all_to_all | solution.py:22
  429.1 16.2 %all-gather.11.cloned.1.call-done = bf16[256,4096]{1,0:T(8,128)(2,1)} async-done(((bf16[256,512]{1,0:T(8,128)(2,1)}), bf16[256,4096]{1,0:T(8,128)(2,1)}) %all-gather.11.cloned.1.call-update) | async-done | bytes 2097168 | tf_op jit(solution)/shard_map/all_gather | solution.py:16
  445.3 2.9 fusion.24
  (303 shorter events, 36.1 us)
Async XLA Ops:
  7.2 19.4 %copy-start.57 = (f32[2,4]{1,0:T(2,128)S(1)}, f32[2,4]{1,0:T(2,128)}, u32[]{:S(2)}) copy-start(f32[2,4]{1,0:T(2,128)} %param.25) | copy-start | bytes 100
  7.2 19.4 %copy-start.61 = (s32[32]{0:T(128)S(1)}, s32[32]{0:T(128)}, u32[]{:S(2)}) copy-start(s32[32]{0:T(128)} %param.16) | copy-start | bytes 388
  7.2 20.1 %copy-start.38 = (f32[2,4,64]{2,1,0:T(4,128)S(1)}, f32[2,4,64]{2,1,0:T(4,128)}, u32[]{:S(2)}) copy-start(f32[2,4,64]{2,1,0:T(4,128)} %param.23) | copy-start | bytes 6148
  7.2 20.1 %copy-start.37 = (f32[2,4,64]{2,1,0:T(4,128)S(1)}, f32[2,4,64]{2,1,0:T(4,128)}, u32[]{:S(2)}) copy-start(f32[2,4,64]{2,1,0:T(4,128)} %param.24) | copy-start | bytes 6148
  7.2 20.8 %copy-start.7 = (f32[2,2,32,256]{3,2,1,0:T(8,128)S(1)}, f32[2,2,32,256]{3,2,1,0:T(8,128)}, u32[]{:S(2)}) copy-start(f32[2,2,32,256]{3,2,1,0:T(8,128)} %param.29) | copy-start | bytes 393220
  7.2 20.8 %copy-start.19 = (f32[2,4096]{1,0:T(2,128)S(1)}, f32[2,4096]{1,0:T(2,128)}, u32[]{:S(2)}) copy-start(f32[2,4096]{1,0:T(2,128)} %param.17) | copy-start | bytes 98308
  7.2 21.4 %copy-start.58 = (f32[2,64]{1,0:T(2,128)S(1)}, f32[2,64]{1,0:T(2,128)}, u32[]{:S(2)}) copy-start(f32[2,64]{1,0:T(2,128)} %param.28) | copy-start | bytes 1540
  7.2 22.3 %copy-start.18 = (bf16[2,256,64]{1,2,0:T(8,128)(2,1)S(1)}, bf16[2,256,64]{1,2,0:T(8,128)(2,1)}, u32[]{:S(2)}) copy-start(bf16[2,256,64]{1,2,0:T(8,128)(2,1)} %param.20) | copy-start | bytes 196612
  7.2 56.5 %all-gather.5.cloned.1.call-start = ((), (), s32[]{:S(2)}) async-start(), calls=%async_computation.14 | async-start | bytes 2359296 | tf_op jit(solution)/shard_map/all_gather | solution.py:16
  22.1 14.8 %all-to-all-start.1 = ((bf16[8,512,64]{1,2,0:T(8,128)(2,1)}), bf16[8,512,64]{1,2,0:T(8,128)(2,1)S(1)}, u32[]{:S(2)}, u32[]{:S(2)}) async-start(bf16[8,512,64]{1,2,0:T(8,128)(2,1)} %broadcast_in_dim.320), calls=%async_computation.1 | async-start | bytes 1048576 | tf_op jit(solution)/shard_map/all_to_all | solution.py:22
  27.2 41.2 %copy-start.29 = (pred[32]{0:T(512)(128)(4,1)}, pred[32]{0:T(512)(128)(4,1)S(1)}, u32[]{:S(2)}) copy-start(pred[32]{0:T(512)(128)(4,1)S(1)} %get-tuple-element.105) | copy-start | bytes 100
  27.2 41.2 %copy-start.32 = (pred[32]{0:T(512)(128)(4,1)}, pred[32]{0:T(512)(128)(4,1)S(1)}, u32[]{:S(2)}) copy-start(pred[32]{0:T(512)(128)(4,1)S(1)} %get-tuple-element.106) | copy-start | bytes 100
  27.2 41.2 %copy-start.44 = (pred[32]{0:T(512)(128)(4,1)}, pred[32]{0:T(512)(128)(4,1)S(1)}, u32[]{:S(2)}) copy-start(pred[32]{0:T(512)(128)(4,1)S(1)} %get-tuple-element.104) | copy-start | bytes 100
  27.2 41.2 %copy-start.46 = (pred[32]{0:T(512)(128)(4,1)}, pred[32]{0:T(512)(128)(4,1)S(1)}, u32[]{:S(2)}) copy-start(pred[32]{0:T(512)(128)(4,1)S(1)} %get-tuple-element.107) | copy-start | bytes 100
  27.2 41.2 %copy-start.49 = (pred[32]{0:T(512)(128)(4,1)}, pred[32]{0:T(512)(128)(4,1)S(1)}, u32[]{:S(2)}) copy-start(pred[32]{0:T(512)(128)(4,1)S(1)} %get-tuple-element.108) | copy-start | bytes 100
  27.2 41.2 %copy-start.52 = (pred[32]{0:T(512)(128)(4,1)}, pred[32]{0:T(512)(128)(4,1)S(1)}, u32[]{:S(2)}) copy-start(pred[32]{0:T(512)(128)(4,1)S(1)} %get-tuple-element.109) | copy-start | bytes 100
  27.2 41.5 %copy-start.26 = (pred[32]{0:T(512)(128)(4,1)}, pred[32]{0:T(512)(128)(4,1)S(1)}, u32[]{:S(2)}) copy-start(pred[32]{0:T(512)(128)(4,1)S(1)} %get-tuple-element.103) | copy-start | bytes 100
  27.2 43.7 %copy-start.20 = (pred[32]{0:T(512)(128)(4,1)}, pred[32]{0:T(512)(128)(4,1)S(1)}, u32[]{:S(2)}) copy-start(pred[32]{0:T(512)(128)(4,1)S(1)} %get-tuple-element.102) | copy-start | bytes 100
  28.6 37.4 %copy-start.42 = (f32[1,4096]{1,0:T(1,128)}, f32[1,4096]{1,0:T(1,128)S(1)}, u32[]{:S(2)}) copy-start(f32[1,4096]{1,0:T(1,128)S(1)} %get-tuple-element.89) | copy-start | bytes 49156
  29.6 41.3 %copy-start.16 = (f32[1,4,64]{2,1,0:T(4,128)}, f32[1,4,64]{2,1,0:T(4,128)S(1)}, u32[]{:S(2)}) copy-start(f32[1,4,64]{2,1,0:T(4,128)S(1)} %get-tuple-element.94) | copy-start | bytes 3076
  37.6 34.6 %all-to-all-start.3 = ((bf16[8,256,64]{1,2,0:T(8,128)(2,1)}), bf16[8,256,64]{1,2,0:T(8,128)(2,1)S(1)}, u32[]{:S(2)}, u32[]{:S(2)}) async-start(bf16[8,256,64]{1,2,0:T(8,128)(2,1)} %broadcast_in_dim.330), calls=%async_computation.3 | async-start | bytes 524288 | tf_op jit(solution)/shard_map/all_to_all | solution.py:22
  71.8 9.1 %copy-start.15 = (bf16[2,256,128]{2,1,0:T(8,128)(2,1)S(1)}, bf16[2,256,128]{2,1,0:T(8,128)(2,1)}, u32[]{:S(2)}) copy-start(bf16[2,256,128]{2,1,0:T(8,128)(2,1)} %param.21) | copy-start | bytes 393220
  73.3 30.7 %all-to-all-start.2 = ((bf16[32,256,64]{1,2,0:T(8,128)(2,1)}), bf16[32,256,64]{1,2,0:T(8,128)(2,1)S(1)}, u32[]{:S(2)}, u32[]{:S(2)}) async-start(bf16[32,256,64]{1,2,0:T(8,128)(2,1)} %broadcast_in_dim.328), calls=%async_computation.2 | async-start | bytes 2097152 | tf_op jit(solution)/shard_map/all_to_all | solution.py:22
  104.9 14.6 %all-to-all-start.5 = ((bf16[8,256,128]{2,1,0:T(8,128)(2,1)}), bf16[8,256,128]{2,1,0:T(8,128)(2,1)S(1)}, u32[]{:S(2)}, u32[]{:S(2)}) async-start(bf16[8,256,128]{2,1,0:T(8,128)(2,1)} %broadcast_in_dim.333), calls=%async_computation.5 | async-start | bytes 1048576 | tf_op jit(solution)/shard_map/all_to_all | solution.py:22
  109.2 17.5 %copy-start.11 = (bf16[2,512,128]{2,1,0:T(8,128)(2,1)S(1)}, bf16[2,512,128]{2,1,0:T(8,128)(2,1)}, u32[]{:S(2)}) copy-start(bf16[2,512,128]{2,1,0:T(8,128)(2,1)} %param.19) | copy-start | bytes 786436
  120.6 33.0 %all-to-all-start.4 = ((bf16[32,256,64]{1,2,0:T(8,128)(2,1)}), bf16[32,256,64]{1,2,0:T(8,128)(2,1)S(1)}, u32[]{:S(2)}, u32[]{:S(2)}) async-start(bf16[32,256,64]{1,2,0:T(8,128)(2,1)} %broadcast_in_dim.331), calls=%async_computation.4 | async-start | bytes 2097152 | tf_op jit(solution)/shard_map/all_to_all | solution.py:22
  154.7 20.3 %copy-start.43 = (f32[1,4096]{1,0:T(1,128)S(1)}, f32[1,4096]{1,0:T(1,128)}, u32[]{:S(2)}) copy-start(f32[1,4096]{1,0:T(1,128)} %copy-done.42) | copy-start | bytes 49156
  154.7 20.3 %all-to-all-start = ((bf16[8,512,128]{2,1,0:T(8,128)(2,1)}), bf16[8,512,128]{2,1,0:T(8,128)(2,1)}, u32[]{:S(2)}, u32[]{:S(2)}) async-start(bf16[8,512,128]{2,1,0:T(8,128)(2,1)} %broadcast_in_dim.317), calls=%async_computation | async-start | bytes 2097152 | tf_op jit(solution)/shard_map/all_to_all | solution.py:22
  159.1 68.3 %all-gather.7.cloned.1.call-start = ((), (), s32[]{:S(2)}) async-start(), calls=%async_computation.15 | async-start | bytes 2359296 | tf_op jit(solution)/shard_map/all_gather | solution.py:16
  175.0 15.4 %copy-start.12 = (bf16[2,512,128]{2,1,0:T(8,128)(2,1)S(1)}, bf16[2,512,128]{2,1,0:T(8,128)(2,1)}, u32[]{:S(2)}) copy-start(bf16[2,512,128]{2,1,0:T(8,128)(2,1)} %param.22) | copy-start | bytes 786436
  190.4 36.9 %copy-start.10 = (bf16[32,8,128]{2,1,0:T(8,128)(2,1)S(1)}, bf16[32,8,128]{2,1,0:T(8,128)(2,1)}, u32[]{:S(2)}) copy-start(bf16[32,8,128]{2,1,0:T(8,128)(2,1)} %param.15) | copy-start | bytes 196612
  192.2 19.4 %all-to-all-start.6 = ((bf16[8,512,128]{2,1,0:T(8,128)(2,1)}), bf16[8,512,128]{2,1,0:T(8,128)(2,1)S(1)}, u32[]{:S(2)}, u32[]{:S(2)}) async-start(bf16[8,512,128]{2,1,0:T(8,128)(2,1)} %broadcast_in_dim.335), calls=%async_computation.6 | async-start | bytes 2097152 | tf_op jit(solution)/shard_map/all_to_all | solution.py:22
  195.8 85.8 %all-gather.9.cloned.1.call-start = ((), (), s32[]{:S(2)}) async-start(), calls=%async_computation.16 | async-start | bytes 2359296 | tf_op jit(solution)/shard_map/all_gather | solution.py:16
  227.3 20.9 %copy-start.56 = (f32[64]{0:T(128)S(1)}, f32[64]{0:T(128)}, u32[]{:S(2)}) copy-start(f32[64]{0:T(128)} %get-tuple-element.2) | copy-start | bytes 772
  243.8 14.6 %all-to-all-start.8 = ((bf16[8,512,64]{1,2,0:T(8,128)(2,1)}), bf16[8,512,64]{1,2,0:T(8,128)(2,1)S(1)}, u32[]{:S(2)}, u32[]{:S(2)}) async-start(bf16[8,512,64]{1,2,0:T(8,128)(2,1)} %broadcast_in_dim.339), calls=%async_computation.8 | async-start | bytes 1048576 | tf_op jit(solution)/shard_map/all_to_all | solution.py:22
  248.1 36.3 %copy-start.40 = (f32[1,4096]{1,0:T(1,128)S(1)}, f32[1,4096]{1,0:T(1,128)}, u32[]{:S(2)}) copy-start(f32[1,4096]{1,0:T(1,128)} %get-tuple-element.88) | copy-start | bytes 49156
  259.1 32.6 %all-to-all-start.10 = ((bf16[8,256,64]{1,2,0:T(8,128)(2,1)}), bf16[8,256,64]{1,2,0:T(8,128)(2,1)S(1)}, u32[]{:S(2)}, u32[]{:S(2)}) async-start(bf16[8,256,64]{1,2,0:T(8,128)(2,1)} %broadcast_in_dim.342), calls=%async_computation.10 | async-start | bytes 524288 | tf_op jit(solution)/shard_map/all_to_all | solution.py:22
  291.7 32.3 %copy-start.9 = (bf16[256,64]{0,1:T(8,128)(2,1)}, bf16[256,64]{0,1:T(8,128)(2,1)S(1)}, u32[]{:S(2)}) copy-start(bf16[256,64]{0,1:T(8,128)(2,1)S(1)} %fusion.87) | copy-start | bytes 98308
  324.1 14.7 %all-to-all-start.12 = ((bf16[8,256,128]{2,1,0:T(8,128)(2,1)}), bf16[8,256,128]{2,1,0:T(8,128)(2,1)}, u32[]{:S(2)}, u32[]{:S(2)}) async-start(bf16[8,256,128]{2,1,0:T(8,128)(2,1)} %broadcast_in_dim.345), calls=%async_computation.12 | async-start | bytes 1048576 | tf_op jit(solution)/shard_map/all_to_all | solution.py:22
  328.4 43.3 %copy-start.5 = (bf16[512,128]{1,0:T(8,128)(2,1)S(1)}, bf16[512,128]{1,0:T(8,128)(2,1)}, u32[]{:S(2)}) copy-start(bf16[512,128]{1,0:T(8,128)(2,1)} %get-tuple-element.76) | copy-start | bytes 393220
  372.8 20.3 %copy-start.41 = (f32[1,4096]{1,0:T(1,128)S(1)}, f32[1,4096]{1,0:T(1,128)}, u32[]{:S(2)}) copy-start(f32[1,4096]{1,0:T(1,128)} %get-tuple-element.88) | copy-start | bytes 49156
  372.8 20.3 %copy-start.60 = (f32[256]{0:T(256)S(1)}, f32[256]{0:T(256)}, u32[]{:S(2)}) copy-start(f32[256]{0:T(256)} %copy-done.59) | copy-start | bytes 3076
  372.8 20.3 %all-to-all-start.7 = ((bf16[8,512,128]{2,1,0:T(8,128)(2,1)}), bf16[8,512,128]{2,1,0:T(8,128)(2,1)}, u32[]{:S(2)}, u32[]{:S(2)}) async-start(bf16[8,512,128]{2,1,0:T(8,128)(2,1)} %broadcast_in_dim.337), calls=%async_computation.7 | async-start | bytes 2097152 | tf_op jit(solution)/shard_map/all_to_all | solution.py:22
  377.2 68.2 %all-gather.11.cloned.1.call-start = ((), (), s32[]{:S(2)}) async-start(), calls=%async_computation.17 | async-start | bytes 2359296 | tf_op jit(solution)/shard_map/all_gather | solution.py:16
  393.1 15.4 %copy-start.6 = (bf16[512,128]{1,0:T(8,128)(2,1)S(1)}, bf16[512,128]{1,0:T(8,128)(2,1)}, u32[]{:S(2)}) copy-start(bf16[512,128]{1,0:T(8,128)(2,1)} %get-tuple-element.74) | copy-start | bytes 393220
  395.8 17.4 %copy-start.17 = (f32[1,4,64]{2,1,0:T(4,128)S(1)}, f32[1,4,64]{2,1,0:T(4,128)}, u32[]{:S(2)}) copy-start(f32[1,4,64]{2,1,0:T(4,128)} %copy-done.16) | copy-start | bytes 3076
  409.7 19.4 %all-to-all-start.13 = ((bf16[8,512,128]{2,1,0:T(8,128)(2,1)}), bf16[8,512,128]{2,1,0:T(8,128)(2,1)S(1)}, u32[]{:S(2)}, u32[]{:S(2)}) async-start(bf16[8,512,128]{2,1,0:T(8,128)(2,1)} %broadcast_in_dim.347), calls=%async_computation.13 | async-start | bytes 2097152 | tf_op jit(solution)/shard_map/all_to_all | solution.py:22
  422.0 23.3 %copy-start.4 = (bf16[256,128]{1,0:T(8,128)(2,1)S(1)}, bf16[256,128]{1,0:T(8,128)(2,1)}, u32[]{:S(2)}) copy-start(bf16[256,128]{1,0:T(8,128)(2,1)} %copy-done.3) | copy-start | bytes 196612
  (30 other events, 86.9 us)
Sparse Core Ops, SparseCore 0:
  20.4 43.3 all-gather.4
  190.5 36.7 all-gather.6
  243.1 38.4 all-gather.8
  408.6 36.6 all-gather.10
where the time goes:
time: 457 us; the launch traced here: 455 us
  waiting for transfers between devices  208 us (46%)
  blocking collectives  114 us (25%)
  starting transfers between devices  54 us (12%)
  local copies, waits for them, and re-layouts  31.5 us (7%)
  matrix products  23.1 us (5%)
  between operations  14.9 us (3%)
  other arithmetic  8.84 us (2%)
    all_to_all x12, waiting for transfers between devices, copy_for_each(): lax.all_to_all(jnp.broadcast_to(array[None], (size, *array.shape)), axis,...  135 us
    all_gather x4, waiting for transfers between devices, gathered_by_axis(): nearer = lax.all_gather(array, axes[-1], axis=dim, tiled=True)  73.5 us
    all_to_all x2, blocking collectives, copy_for_each(): lax.all_to_all(jnp.broadcast_to(array[None], (size, *array.shape)), axis,...  63.3 us
    all_to_all x12, starting transfers between devices, copy_for_each(): lax.all_to_all(jnp.broadcast_to(array[None], (size, *array.shape)), axis,...  53.9 us
    all_gather x4, blocking collectives, gathered_by_axis(): nearer = lax.all_gather(array, axes[-1], axis=dim, tiled=True)  51 us
    dot_general x10, matrix products, project(): jnp.dot(gathered, gather_directly(weight, 'dp', 0), preferred_element_typ...  16.6 us
    broadcast_in_dim x19, local copies, waits for them, and re-layouts, copy_for_each(): jnp.broadcast_to(array[None], (size, *array.shape))  15.5 us
  transfers between devices with their start and end apart: 16, of which 14 were waited for; matrix products, arithmetic and copies ran while one was open for 10% of the time, Pallas kernels for 0%

commit v1 on v0

v1 whole, which is shorter than its diff:
```python
import functools
import math

import jax
import jax.numpy as jnp
from jax import lax
from jax.experimental import pallas as pl
from jax.experimental.pallas import tpu as pltpu
from jax.sharding import PartitionSpec as P

MESH = pl.DeviceIdType.MESH
HIGH = lax.Precision.HIGHEST
EPS = 1e-05
NZ, NX, NY = 8, 4, 4
LANES = 128
F32, BF16 = jnp.float32, jnp.bfloat16
NT = (((1,), (1,)), ((), ()))
PIECES = 7


def dot(a, b, **kw):
    return jnp.dot(a, b, preferred_element_type=F32, **kw)


def dot_nt(a, b):
    return lax.dot_general(a, b, NT, preferred_element_type=F32)


def iota(shape, dim):
    return lax.broadcasted_iota(jnp.int32, shape, dim)


def ones_where(cond, dtype=BF16):
    return jnp.where(cond, 1.0, 0.0).astype(dtype)


def swap_halves(value):
    return pltpu.roll(value, 64, 1)


class Place:
    def __init__(self):
        self.tp = lax.axis_index("tp")
        self.dp = lax.axis_index("dp")
        self.z, self.x = self.tp // NX, self.tp % NX
        self.y, self.core = self.dp // 2, self.dp % 2

    def at_x(self, step):
        return (self.z * NX + (self.x + step) % NX, self.dp)

    def at_z(self, step):
        return ((self.z + step) % NZ * NX + self.x, self.dp)

    def at_y(self, step):
        return (self.tp, (self.y + step) % NY * 2 + self.core)

    def partner(self):
        return (self.tp, self.y * 2 + 1 - self.core)


def remote(ref, send, recv, device):
    return pltpu.make_async_remote_copy(
        src_ref=ref, dst_ref=ref, send_sem=send, recv_sem=recv, device_id=device, device_id_type=MESH
    )


class Gather:
    def __init__(self, place, buf, rows, send, recv):
        self.p, self.buf, self.send, self.recv = place, buf, send, recv
        self.half, self.quarter = rows // 2, rows // 4
        self.sent = []

    def lane(self, step=0):
        return pl.ds(pl.multiple_of((self.p.x + step) % NX * LANES, LANES), LANES)

    def row(self, step):
        return (self.p.z + step) % NZ

    def upper(self, step, x_step=None):
        lanes = slice(None) if x_step is None else self.lane(x_step)
        return self.buf.at[self.row(step), pl.ds(0, self.half), lanes]

    def lower(self, step):
        return self.buf.at[self.row(step), pl.ds(self.half, self.half), self.lane()]

    def lower_column(self, x_step):
        return self.buf.at[:, pl.ds(self.half, self.half), self.lane(x_step)]

    def part(self, step, which):
        return self.buf.at[self.row(step), pl.ds(which * self.quarter, self.quarter), :]

    def go(self, ref, index, device):
        copy = remote(ref, self.send.at[index], self.recv.at[index], device)
        copy.start()
        self.sent.append(copy)

    def arrive(self, ref, index):
        remote(ref, self.send.at[index], self.recv.at[index], self.p.partner()).wait_recv()

    def put(self, value):
        self.buf[self.p.z, :, self.lane()] = value

    def start(self):
        for d in range(1, NX):
            self.go(self.upper(0, 0), d - 1, self.p.at_x(d))
        for d in range(1, NZ):
            self.go(self.lower(0), 2 + d, self.p.at_z(d))

    def middle(self):
        for d in range(1, NX):
            self.arrive(self.upper(0, NX - d), d - 1)
        self.go(self.upper(0), 10, self.p.at_z(1))
        self.go(self.upper(0), 14, self.p.at_z(NZ - 1))
        for d in range(1, NZ):
            self.arrive(self.lower(NZ - d), 2 + d)
        for d in range(1, NX):
            self.go(self.lower_column(0), 17 + d, self.p.at_x(d))

    def ring(self):
        for s in range(1, 4):
            self.arrive(self.upper(NZ - s), 9 + s)
            ref = self.upper(NZ - s) if s < 3 else self.part(NZ - s, 0)
            self.go(ref, 10 + s, self.p.at_z(1))
            self.arrive(self.upper(s), 13 + s)
            ref = self.upper(s) if s < 3 else self.part(s, 1)
            self.go(ref, 14 + s, self.p.at_z(NZ - 1))

    def finish(self):
        self.arrive(self.part(4, 0), 13)
        self.arrive(self.part(4, 1), 17)
        for d in range(1, NX):
            self.arrive(self.lower_column(NX - d), 17 + d)
        for copy in self.sent:
            copy.wait_send()


class Weights:
    def __init__(self, place, wdo, wg, wm, we, y_send, y_recv, c_send, c_recv):
        self.p = place
        self.refs = (wdo, wg, wm, we)
        self.sems = (y_send, y_recv, c_send, c_recv)
        self.sent = []

    def region(self, piece, shard):
        wdo, wg, wm, we = self.refs
        if piece in (0, 3, 4, 6):
            rows = pl.ds(pl.multiple_of(shard * 512, 512), 512)
        else:
            rows = pl.ds(pl.multiple_of(shard * 256, 256), 256)
        if piece == 0:
            return wdo.at[rows, pl.ds(0, 256)]
        if piece == 4:
            return wdo.at[rows, pl.ds(256, 128)]
        if piece == 1:
            return wg.at[rows, :]
        if piece in (2, 5):
            return wm.at[(piece - 2) // 3, rows, :]
        return we.at[(piece - 3) // 3, rows, :]

    def like(self, step):
        return (self.p.y + step) % NY * 2 + self.p.core

    def unlike(self, step):
        return (self.p.y + step) % NY * 2 + 1 - self.p.core

    def y_copy(self, piece, d, shard):
        y_send, y_recv, _, _ = self.sems
        return remote(self.region(piece, shard), y_send.at[piece, d - 1], y_recv.at[piece, d - 1], self.p.at_y(d))

    def c_copy(self, piece, d, shard):
        _, _, c_send, c_recv = self.sems
        return remote(self.region(piece, shard), c_send.at[piece, d], c_recv.at[piece, d], self.p.partner())

    def begin(self, copy):
        copy.start()
        self.sent.append(copy)

    def start(self, piece):
        for d in (1, 3, 2):
            self.begin(self.y_copy(piece, d, self.p.dp))
        self.begin(self.c_copy(piece, 0, self.p.dp))

    def forward(self, piece):
        for d in (1, 3, 2):
            shard = self.like(NY - d)
            self.y_copy(piece, d, shard).wait_recv()
            self.begin(self.c_copy(piece, d, shard))

    def finish(self, piece):
        for d in range(NY):
            self.c_copy(piece, d, self.unlike((NY - d) % NY)).wait_recv()

    def drain(self):
        for copy in self.sent:
            copy.wait_send()


def kernel(
    rows,
    tokens,
    lengths,
    gains,
    drive,
    opening,
    glu,
    merge,
    leaving,
    decay,
    turn,
    step,
    s_in,
    s_out,
    skip,
    carried,
    out_tokens,
    out_state,
    wdo,
    wg,
    wm,
    we,
    gp,
    mp,
    gx,
    ga,
    pick,
    spread_seq,
    spread_slot,
    live,
    params,
    inject,
    readout_w,
    pushed,
    trail,
    y_send,
    y_recv,
    c_send,
    c_recv,
    g_send,
    g_recv,
):
    place = Place()
    half = rows // 2
    barrier = pltpu.get_barrier_semaphore()
    peers = [place.at_x(d) for d in range(1, NX)] + [place.at_z(d) for d in range(1, NZ)]
    peers += [place.at_y(d) for d in range(1, NY)] + [place.partner()]
    for peer in peers:
        pl.semaphore_signal(barrier, inc=1, device_id=peer, device_id_type=MESH)

    def gather(index):
        wide = index in (0, 3)
        return wide

    gathers = []
    for g in range(8):
        layer, kind = g // 4, g % 4
        if kind in (0, 3):
            buf, n = gx.at[layer * 2 + kind // 3], rows
        else:
            buf, n = ga.at[layer * 2 + kind - 1], half
        gathers.append(Gather(place, buf, n, g_send.at[g], g_recv.at[g]))
    weights = Weights(place, wdo, wg, wm, we, y_send, y_recv, c_send, c_recv)

    lens = lengths[...].astype(F32)
    lens_rows = jnp.broadcast_to(lens, (256, 32)).astype(BF16)
    seq, col = iota((32, 256), 0), iota((32, 256), 1)
    by_seq = lax.shift_right_logical(col, 3)
    off = dot(lens_rows[0:8], ones_where(seq < by_seq))[0:1]
    size = dot(lens_rows[0:8], ones_where(seq == by_seq))[0:1]
    slot = jnp.bitwise_and(iota((1, 256), 1), 7).astype(F32)
    target = jnp.where(slot < size, off + slot, -1.0)
    compact = ones_where(iota((rows, 256), 0).astype(F32) == target)
    residual = dot(compact, tokens[...]).astype(BF16)
    gathers[0].put(residual)

    own512 = pl.ds(pl.multiple_of(place.dp * 512, 512), 512)
    own256 = pl.ds(pl.multiple_of(place.dp * 256, 256), 256)
    wdo[own512, 0:128] = opening[0]
    wdo[own512, 128:256] = jnp.concatenate([drive[0], drive[1]], axis=1)
    wdo[own512, 256:384] = opening[1]
    wg[own256, :] = jnp.concatenate([glu[0], glu[1]], axis=1)
    for layer in range(2):
        wm[layer, own256, :] = merge[layer]
        we[layer, own512, :] = leaving[layer]

    pl.semaphore_wait(barrier, len(peers))
    gathers[0].start()
    for piece in range(PIECES):
        weights.start(piece)

    by_slot_seq = jnp.bitwise_and(col, 31)
    off = dot(lens_rows[0:8], ones_where(seq < by_slot_seq))[0:1]
    size = dot(lens_rows[0:8], ones_where(seq == by_slot_seq))[0:1]
    slot = lax.shift_right_logical(iota((1, 256), 1), 5).astype(F32)
    target = jnp.where(slot < size, off + slot, -1.0)
    pick[...] = ones_where(iota((rows, 256), 0).astype(F32) == target)
    row, other = iota((256, 32), 0), iota((256, 32), 1)
    place_of_row = iota((256, rows), 1).astype(F32)
    lens_many = jnp.broadcast_to(lens, (256, 32)).astype(BF16)
    for order, ref in ((0, spread_seq), (1, spread_slot)):
        if order == 0:
            which = lax.shift_right_logical(row, 3)
            at = jnp.bitwise_and(iota((256, 256), 0), 7).astype(F32)
        else:
            which = jnp.bitwise_and(row, 31)
            at = lax.shift_right_logical(iota((256, 256), 0), 5).astype(F32)
        off = dot_nt(ones_where(other < which), lens_many)
        size = dot_nt(ones_where(other == which), lens_many)
        target = jnp.where(at < size, off + at, -1.0)
        ref[...] = ones_where(place_of_row == target[:, 0:rows])
        live[order] = ones_where(at < size, F32)

    gathers[0].middle()

    spread64 = ones_where(iota((64, 256), 0) == jnp.bitwise_and(iota((64, 256), 1), 63), F32)
    spread16 = ones_where(iota((16, 128), 0) == jnp.bitwise_and(iota((16, 128), 1), 15), F32)
    spread2 = ones_where(iota((64, 128), 0) == jnp.bitwise_and(iota((64, 128), 1), 63), F32)
    group4 = iota((4, 256), 0) == lax.shift_right_logical(iota((4, 256), 1), 6)
    size_all = dot(step[...], ones_where(group4, F32), precision=HIGH)
    skip_all = dot(skip[...], spread2, precision=HIGH)
    for layer in range(2):
        rate = dot(decay[layer], spread64, precision=HIGH)
        rate = jnp.sum(jnp.where(group4, rate, 0.0), axis=0, keepdims=True)
        turning = dot(turn[layer], spread64, precision=HIGH)
        turning = jnp.sum(jnp.where(group4, turning, 0.0), axis=0, keepdims=True)
        length = size_all[layer : layer + 1]
        real = -rate
        magnitude = jnp.exp(length * real)
        decay_real = magnitude * jnp.cos(length * turning)
        decay_imag = magnitude * jnp.sin(length * turning)
        divisor = real * real + turning * turning
        params[layer, 0:1, :] = decay_real
        params[layer, 1:2, :] = decay_imag
        params[layer, 2:3, :] = ((decay_real - 1.0) * real + decay_imag * turning) / divisor
        params[layer, 3:4, :] = (decay_imag * real - (decay_real - 1.0) * turning) / divisor
        params[layer, 4:5, 0:128] = skip_all[layer : layer + 1]
        in_group = lax.shift_right_logical(iota((256, 128), 0), 6) == jnp.bitwise_and(
            lax.shift_right_logical(iota((256, 128), 1), 4), 3
        )
        out_group = lax.shift_right_logical(iota((64, 256), 0), 4) == lax.shift_right_logical(
            iota((64, 256), 1), 6
        )
        for part in range(2):
            wide = jnp.where(in_group, dot(s_in[layer, part], spread16, precision=HIGH), 0.0)
            high = wide.astype(BF16)
            inject[layer, part * 256 : part * 256 + 256, 0:128] = high
            inject[layer, part * 256 : part * 256 + 256, 128:256] = (wide - high.astype(F32)).astype(BF16)
            wide = jnp.where(out_group, dot(s_out[layer, part], spread64, precision=HIGH), 0.0)
            wide = (wide if part == 0 else -wide).astype(BF16)
            readout_w[layer, 0:64, part * 256 : part * 256 + 256] = wide
            readout_w[layer, 64:128, part * 256 : part * 256 + 256] = wide

    lane = iota((rows, 128), 1)
    lane_half = iota((half, 128), 1)
    low256 = iota((256, 128), 1) < 64

    def build_gp():
        zero = jnp.zeros((256, 128), BF16)
        for k in range(8):
            plain = wg[k * 256 : k * 256 + 256, :]
            turned = swap_halves(plain.astype(F32)).astype(BF16)
            for layer in range(2):
                first, second = (plain, turned) if layer == 0 else (turned, plain)
                top = jnp.where(low256, first, zero).reshape(4, 64, 128)
                bottom = jnp.where(low256, zero, second).reshape(4, 64, 128)
                gp[layer, k * 512 : k * 512 + 512, :] = jnp.concatenate([top, bottom], axis=1).reshape(512, 128)

    def build_mp(layer):
        zero = jnp.zeros((4, 64, 128), BF16)
        for k in range(8):
            plain = wm[layer, k * 256 : k * 256 + 256, :].reshape(4, 64, 128)
            mp[layer, k * 512 : k * 512 + 512, 0:128] = jnp.concatenate([plain, zero], axis=1).reshape(512, 128)
            mp[layer, k * 512 : k * 512 + 512, 128:256] = jnp.concatenate([zero, plain], axis=1).reshape(512, 128)

    def project(buf, weight):
        total = None
        for k in range(NZ):
            term = dot(buf[k], weight(k * 512, 512))
            total = term if total is None else total + term
        return total

    for layer in range(2):
        first = gathers[layer * 4]
        first.ring()
        if layer == 0:
            weights.forward(0)
        else:
            weights.finish(4)
        first.finish()
        if layer == 0:
            weights.finish(0)
        squares = None
        for k in range(NZ):
            value = first.buf[k].astype(F32)
            term = jnp.sum(value * value, axis=1, keepdims=True)
            squares = term if squares is None else squares + term
        inverse = lax.rsqrt(squares / (NZ * 512.0) + EPS)
        total = None
        for k in range(NZ):
            gain = gains[layer : layer + 1, k * 512 : k * 512 + 512]
            normed = (first.buf[k].astype(F32) * inverse * gain).astype(BF16)
            term = dot(normed, wdo[k * 512 : k * 512 + 512, layer * 128 : layer * 128 + 256])
            total = term if total is None else total + term
        lanes_open = slice(0, 128) if layer == 0 else slice(128, 256)
        lanes_drive = slice(128, 256) if layer == 0 else slice(0, 128)
        gate_open = jax.nn.sigmoid(total[:, lanes_open])
        both = total[:, lanes_drive]
        high = both.astype(BF16).astype(F32)
        rest = swap_halves(both - high)
        mine = lane < 64 if layer == 0 else lane >= 64
        split = jnp.where(mine, high, rest).astype(BF16)
        spread = dot(spread_slot[...], split)
        drives = spread + swap_halves(spread)
        spread = spread.astype(BF16)
        moved = dot_nt(jnp.concatenate([spread, spread], axis=1), inject[layer])
        hold_real, hold_imag = params[layer, 2:3, :], params[layer, 3:4, :]
        pushed[:, 0:256] = hold_real * moved[:, 0:256] - hold_imag * moved[:, 256:512]
        pushed[:, 256:512] = hold_real * moved[:, 256:512] + hold_imag * moved[:, 0:256]
        decay_real = jnp.broadcast_to(params[layer, 0:1, :], (32, 256))
        decay_imag = jnp.broadcast_to(params[layer, 1:2, :], (32, 256))
        state_real, state_imag = carried[layer, 0], carried[layer, 1]
        for t in range(8):
            now = slice(t * 32, t * 32 + 32)
            alive = live[1, now, :] > 0.5
            next_real = decay_real * state_real - decay_imag * state_imag + pushed[now, 0:256]
            next_imag = decay_real * state_imag + decay_imag * state_real + pushed[now, 256:512]
            state_real = jnp.where(alive, next_real, state_real)
            state_imag = jnp.where(alive, next_imag, state_imag)
            trail[now, 0:256] = state_real.astype(BF16)
            trail[now, 256:512] = state_imag.astype(BF16)
        out_state[layer, 0] = state_real
        out_state[layer, 1] = state_imag
        readout = dot_nt(trail[...], readout_w[layer]) + params[layer, 4:5, 0:128] * drives
        inner = math.sqrt(2.0 / math.pi) * (readout + 0.044715 * (readout * readout * readout))
        activated = (readout * (0.5 * (1.0 + jnp.tanh(inner)))).astype(BF16)
        top = dot(pick[0:half, :], activated)
        bottom = dot(pick[half:rows, :], activated)
        packed = jnp.where(lane_half < 64, top, bottom)
        second = gathers[layer * 4 + 1]
        second.put(packed.astype(BF16))
        second.start()
        if layer == 0:
            weights.forward(1)
            weights.forward(2)
        second.middle()
        if layer == 0:
            weights.finish(1)
            build_gp()
        second.ring()
        if layer == 0:
            weights.forward(3)
        second.finish()
        gating = project(second.buf, lambda k, n: gp[layer, k : k + n, :])
        gated = (packed * jax.nn.sigmoid(gating)).astype(BF16)
        third = gathers[layer * 4 + 2]
        third.put(gated)
        third.start()
        if layer == 0:
            weights.forward(4)
        third.middle()
        weights.finish(2 + 3 * layer)
        build_mp(layer)
        third.ring()
        third.finish()
        merged = project(third.buf, lambda k, n: mp[layer, k : k + n, :])
        merged = jnp.concatenate([merged[:, 0:128], merged[:, 128:256]], axis=0)
        mixed = (gate_open * merged).astype(BF16)
        fourth = gathers[layer * 4 + 3]
        fourth.put(mixed)
        fourth.start()
        if layer == 0:
            weights.forward(5)
            weights.forward(6)
        fourth.middle()
        fourth.ring()
        weights.finish(3 + 3 * layer)
        fourth.finish()
        branch = project(fourth.buf, lambda k, n: we[layer, k : k + n, :])
        residual = (residual.astype(F32) + branch).astype(BF16)
        if layer == 0:
            following = gathers[4]
            following.put(residual)
            following.start()
            following.middle()

    spread = dot(spread_seq[...], residual).astype(BF16)
    out_tokens[...] = jnp.where(live[0, :, 0:128] > 0.5, spread, tokens[...])
    weights.drain()


def block(rows, number):
    vmem = pl.BlockSpec(memory_space=pltpu.VMEM)
    half = rows // 2
    return pl.pallas_call(
        functools.partial(kernel, rows),
        name=f"layers_{rows}",
        out_shape=(
            jax.ShapeDtypeStruct((256, 128), BF16),
            jax.ShapeDtypeStruct((2, 2, 32, 256), F32),
        ),
        in_specs=[vmem] * 15,
        out_specs=(vmem, vmem),
        scratch_shapes=[
            pltpu.VMEM((4096, 384), BF16),
            pltpu.VMEM((2048, 128), BF16),
            pltpu.VMEM((2, 2048, 128), BF16),
            pltpu.VMEM((2, 4096, 128), BF16),
            pltpu.VMEM((2, 4096, 128), BF16),
            pltpu.VMEM((2, 4096, 256), BF16),
            pltpu.VMEM((4, NZ, rows, 512), BF16),
            pltpu.VMEM((4, NZ, half, 512), BF16),
            pltpu.VMEM((rows, 256), BF16),
            pltpu.VMEM((256, rows), BF16),
            pltpu.VMEM((256, rows), BF16),
            pltpu.VMEM((2, 256, 256), F32),
            pltpu.VMEM((2, 8, 256), F32),
            pltpu.VMEM((2, 512, 256), BF16),
            pltpu.VMEM((2, 128, 512), BF16),
            pltpu.VMEM((256, 512), F32),
            pltpu.VMEM((256, 512), BF16),
            pltpu.SemaphoreType.DMA((PIECES, 3)),
            pltpu.SemaphoreType.DMA((PIECES, 3)),
            pltpu.SemaphoreType.DMA((PIECES, 4)),
            pltpu.SemaphoreType.DMA((PIECES, 4)),
            pltpu.SemaphoreType.DMA((8, 21)),
            pltpu.SemaphoreType.DMA((8, 21)),
        ],
        compiler_params=pltpu.CompilerParams(
            collective_id=number, has_side_effects=True, vmem_limit_bytes=60 * 1024 * 1024
        ),
    )


def shards(tokens, lengths, norm_gains, drive, opening, glu, merge, leaving, decay, turn, step, s_in, s_out, skip, carried):
    arrays = (
        tokens.reshape(256, 128),
        lengths.reshape(1, 32),
        norm_gains,
        drive,
        opening,
        glu,
        merge,
        leaving,
        decay,
        turn,
        step,
        s_in.reshape(2, 2, 256, 16),
        s_out.reshape(2, 2, 64, 64),
        skip,
        carried,
    )
    updated, state = block(256, 0)(*arrays)
    return updated.reshape(32, 8, 128), state


def solution(mesh):
    placed = (
        P("dp", None, "tp"),
        P("dp"),
        P(),
        P(None, "dp", "tp"),
        P(None, "dp", "tp"),
        P(None, "dp", "tp"),
        P(None, "dp", "tp"),
        P(None, "dp", "tp"),
        P(None, "tp", None),
        P(None, "tp", None),
        P(None, "tp"),
        P(None, None, "tp", None, None),
        P(None, None, "tp", None, None),
        P(None, "tp"),
        P(None, None, "dp", "tp"),
    )
    return jax.shard_map(
        shards,
        mesh=mesh,
        in_specs=placed,
        out_specs=(P("dp", None, "tp"), P(None, None, "dp", "tp")),
        check_vma=False,
    )
```

time: 457 us -> 199 us (0.44)
  waiting for transfers between devices: 208 us -> 0 us
  Pallas kernels: 0 us -> 191 us
  blocking collectives: 114 us -> 0 us
  starting transfers between devices: 54 us -> 0 us
  local copies, waits for them, and re-layouts: 31.5 us -> 5.71 us
  matrix products: 23.1 us -> 0 us
  between operations: 14.9 us -> 0.66 us
  other arithmetic: 8.84 us -> 0 us
    pallas_call x0 -> x1, Pallas kernels: none -> 191 us  [shards(): updated, state = block(256, 0)(*arrays)]
    all_to_all x12 -> x0, waiting for transfers between devices: 135 us -> none  [copy_for_each(): lax.all_to_all(jnp.broadcast_to(array[None], (size, *array.shape)), axis,...]
    all_gather x4 -> x0, waiting for transfers between devices: 73.5 us -> none  [gathered_by_axis(): nearer = lax.all_gather(array, axes[-1], axis=dim, tiled=True)]
    all_to_all x2 -> x0, blocking collectives: 63.3 us -> none  [copy_for_each(): lax.all_to_all(jnp.broadcast_to(array[None], (size, *array.shape)), axis,...]
    all_to_all x12 -> x0, starting transfers between devices: 53.9 us -> none  [copy_for_each(): lax.all_to_all(jnp.broadcast_to(array[None], (size, *array.shape)), axis,...]
    all_gather x4 -> x0, blocking collectives: 51 us -> none  [gathered_by_axis(): nearer = lax.all_gather(array, axes[-1], axis=dim, tiled=True)]
    dot_general x46 -> x0, matrix products: 23.1 us -> none  [the longest x10 16.6 us: project(): jnp.dot(gathered, gather_directly(weight, 'dp', 0), preferred_element_typ...]
    broadcast_in_dim x19 -> x0, local copies, waits for them, and re-layouts: 15.5 us -> none  [copy_for_each(): jnp.broadcast_to(array[None], (size, *array.shape))]
  transfers between devices with their start and end apart: 16 -> 0, of which waited for: 14 -> 0; matrix products, arithmetic and copies ran while one was open for 10% -> 0% of each run, Pallas kernels for 0% -> 0%
where the time goes in v1:
time: 199 us; the launch traced here: 197 us
  Pallas kernels  191 us (96%)
  local copies, waits for them, and re-layouts  5.71 us (3%)
    pallas_call x1, Pallas kernels, shards(): updated, state = block(256, 0)(*arrays)  191 us
    unnamed x11, local copies, waits for them, and re-layouts  5.71 us

profile of v1, /device:TPU:32, one launch (start us, length us, event | category | flops | bytes accessed | tf_op | source)
XLA Modules:
  0.0 197.4 jit_solution(11307878752276162347)
XLA Ops:
  0.6 0.0 copy-start
  0.6 1.6 copy.19.glu
  2.3 0.0 copy-done
  2.3 0.0 copy-start.1
  2.3 0.8 copy.18.drive
  3.1 0.1 copy-done.1
  3.2 1.0 copy.17
  4.2 191.0 %layers_256.1 = (bf16[256,128]{1,0:T(8,128)(2,1)}, f32[2,2,32,256]{3,2,1,0:T(8,128)}) custom-call(bf16[256,128]{1,0:T(8,128)(2,1)} %bitcast.7, s32[1,32]{1,0:T(1,128)} %bitcast.9, f32[2,4096]{1,0:T(2,128)} %gains.1, bf16[2,512,64]{2,1,0:T(8,128)(2,1)} %copy.18.drive, bf16[2,512,128]{2,1,0:T(8,128)(2,1)} %opening.1, bf16[2,256,64]{2,1,0:T(8,128)(2,1)} %copy.19.glu, ...), custom_call_target="tpu_custom_call" | custom-call | tf_op jit(solution)/shard_map/layers_256/pallas_call | solution.py:551
  195.2 0.0 copy-start.2
  195.2 1.5 copy.22
  196.7 0.0 copy-done.2
  196.7 0.7 copy.23
Async XLA Ops:
  0.6 1.6 copy-start
  2.3 0.9 copy-start.1
  195.2 1.5 copy-start.2

commit v2 on v1

v2 whole, which is shorter than its diff:
```python
import math

import jax
import jax.numpy as jnp
from jax import lax
from jax.experimental import pallas as pl
from jax.experimental.pallas import tpu as pltpu
from jax.sharding import PartitionSpec as P

MESH = pl.DeviceIdType.MESH
HIGH = lax.Precision.HIGHEST
EPS = 1e-05
NZ, NX, NY, NDP = 8, 4, 4, 8
Z_ORDER, X_ORDER = (1, 7, 2, 6, 3, 5, 4), (1, 3, 2)
ROWS, STREAMS = 128, 1
PART = ROWS // STREAMS
LANES = 128
F32, BF16 = jnp.float32, jnp.bfloat16
NT = (((1,), (1,)), ((), ()))
PIECES = 7


def dot(a, b, **kw):
    return jnp.dot(a, b, preferred_element_type=F32, **kw)


def dot_nt(a, b):
    return lax.dot_general(a, b, NT, preferred_element_type=F32)


def iota(shape, dim):
    return lax.broadcasted_iota(jnp.int32, shape, dim)


def ones_where(cond, dtype=BF16):
    return jnp.where(cond, 1.0, 0.0).astype(dtype)


def swap_halves(value):
    return pltpu.roll(value, 64, 1)


class Place:
    def __init__(self):
        self.tp = lax.axis_index("tp")
        self.dp = lax.axis_index("dp")
        self.z, self.x = self.tp // NX, self.tp % NX
        self.y, self.core = self.dp // 2, self.dp % 2

    def at_x(self, step):
        return (self.z * NX + (self.x + step) % NX, self.dp)

    def at_z(self, step):
        return ((self.z + step) % NZ * NX + self.x, self.dp)

    def at_y(self, step):
        return (self.tp, (self.y + step) % NY * 2 + self.core)

    def at_dp(self, step):
        return (self.tp, (self.dp + step) % NDP)

    def partner(self):
        return (self.tp, self.y * 2 + 1 - self.core)


def remote(ref, send, recv, device):
    return pltpu.make_async_remote_copy(
        src_ref=ref, dst_ref=ref, send_sem=send, recv_sem=recv, device_id=device, device_id_type=MESH
    )


class Gather:
    def __init__(self, place, buf, send, recv):
        self.p, self.buf, self.send, self.recv = place, buf, send, recv
        self.sent = []

    def block(self, dz, dx):
        lanes = pl.ds(pl.multiple_of((self.p.x + dx) % NX * LANES, LANES), LANES)
        return self.buf.at[(self.p.z + dz) % NZ, :, lanes]

    def go(self, ref, index, device):
        copy = remote(ref, self.send.at[index], self.recv.at[index], device)
        copy.start()
        self.sent.append(copy)

    def arrive(self, ref, index):
        remote(ref, self.send.at[index], self.recv.at[index], self.p.partner()).wait_recv()

    def put(self, value):
        lanes = pl.ds(pl.multiple_of(self.p.x * LANES, LANES), LANES)
        self.buf[self.p.z, :, lanes] = value

    def start(self):
        for d in Z_ORDER:
            self.go(self.block(0, 0), d - 1, self.p.at_z(d))
        for e in X_ORDER:
            self.go(self.block(0, 0), 6 + e, self.p.at_x(e))

    def forward(self, d):
        ref = self.block(NZ - d, 0)
        self.arrive(ref, d - 1)
        for e in X_ORDER:
            self.go(ref, 6 + d * 3 + e, self.p.at_x(e))

    def finish(self):
        for e in X_ORDER:
            self.arrive(self.block(0, NX - e), 6 + e)
        for d in Z_ORDER:
            for e in X_ORDER:
                self.arrive(self.block(NZ - d, NX - e), 6 + d * 3 + e)
        for copy in self.sent:
            copy.wait_send()


class Weights:
    def __init__(self, place, wdo, wg, wm, we, y_send, y_recv, c_send, c_recv):
        self.p = place
        self.refs = (wdo, wg, wm, we)
        self.sems = (y_send, y_recv, c_send, c_recv)
        self.sent = []

    def region(self, piece, shard):
        wdo, wg, wm, we = self.refs
        if piece in (0, 3, 4, 6):
            rows = pl.ds(pl.multiple_of(shard * 512, 512), 512)
        else:
            rows = pl.ds(pl.multiple_of(shard * 256, 256), 256)
        if piece == 0:
            return wdo.at[rows, pl.ds(0, 256)]
        if piece == 4:
            return wdo.at[rows, pl.ds(256, 128)]
        if piece == 1:
            return wg.at[rows, :]
        if piece in (2, 5):
            return wm.at[(piece - 2) // 3, rows, :]
        return we.at[(piece - 3) // 3, rows, :]

    def like(self, step):
        return (self.p.y + step) % NY * 2 + self.p.core

    def unlike(self, step):
        return (self.p.y + step) % NY * 2 + 1 - self.p.core

    def y_copy(self, piece, d, shard):
        y_send, y_recv, _, _ = self.sems
        return remote(self.region(piece, shard), y_send.at[piece, d - 1], y_recv.at[piece, d - 1], self.p.at_y(d))

    def c_copy(self, piece, d, shard):
        _, _, c_send, c_recv = self.sems
        return remote(self.region(piece, shard), c_send.at[piece, d], c_recv.at[piece, d], self.p.partner())

    def begin(self, copy):
        copy.start()
        self.sent.append(copy)

    def start(self, piece):
        for d in (1, 3, 2):
            self.begin(self.y_copy(piece, d, self.p.dp))
        self.begin(self.c_copy(piece, 0, self.p.dp))

    def forward(self, piece):
        for d in (1, 3, 2):
            shard = self.like(NY - d)
            self.y_copy(piece, d, shard).wait_recv()
            self.begin(self.c_copy(piece, d, shard))

    def finish(self, piece):
        for d in range(NY):
            self.c_copy(piece, d, self.unlike((NY - d) % NY)).wait_recv()

    def drain(self):
        for copy in self.sent:
            copy.wait_send()


def kernel(
    tokens,
    lengths,
    base,
    gains,
    drive,
    opening,
    glu,
    merge,
    leaving,
    decay,
    turn,
    step,
    s_in,
    s_out,
    skip,
    carried,
    out_tokens,
    out_state,
    out_count,
    wdo,
    wg,
    wm,
    we,
    gp,
    mp,
    gx,
    ga,
    pick,
    spread_seq,
    spread_slot,
    live_seq,
    live_slot,
    params,
    inject,
    readout_w,
    pushed,
    trail,
    counts,
    y_send,
    y_recv,
    c_send,
    c_recv,
    g_send,
    g_recv,
    n_send,
    n_recv,
):
    place = Place()
    half = PART // 2
    barrier = pltpu.get_barrier_semaphore()
    peers = [place.at_x(d) for d in range(1, NX)] + [place.at_z(d) for d in range(1, NZ)]
    peers += [place.at_dp(d) for d in range(1, NDP)]
    for peer in peers:
        pl.semaphore_signal(barrier, inc=1, device_id=peer, device_id_type=MESH)

    gathers = {}
    for layer in range(2):
        for kind in range(4):
            for s in range(STREAMS):
                ref = (gx.at[layer, kind // 3, s]) if kind in (0, 3) else ga.at[layer, kind - 1, s]
                index = (layer * 4 + kind) * STREAMS + s
                gathers[layer, kind, s] = Gather(place, ref, g_send.at[index], g_recv.at[index])
    weights = Weights(place, wdo, wg, wm, we, y_send, y_recv, c_send, c_recv)

    lens = lengths[...].astype(F32)
    lens_rows = jnp.broadcast_to(lens, (256, 32)).astype(BF16)
    seq, col = iota((32, 256), 0), iota((32, 256), 1)
    row, other = iota((256, 256), 0), iota((256, 256), 1)
    size_slot = dot(lens_rows, ones_where(seq == jnp.bitwise_and(col, 31)))
    is_live_slot = lax.shift_right_logical(other, 5).astype(F32) < size_slot
    counted = ones_where(is_live_slot)
    size_seq = dot(lens_rows[0:8], ones_where(seq == lax.shift_right_logical(col, 3)))[0:1]
    is_live_seq = jnp.bitwise_and(iota((1, 256), 1), 7).astype(F32) < size_seq
    rank_seq = jnp.bitwise_and(other, 7) * 32 + lax.shift_right_logical(other, 3)
    number_seq = dot(counted[0:8], ones_where(row < rank_seq))[0:1]
    origin = base[...]
    target = jnp.where(is_live_seq, number_seq - origin, -1.0)
    residuals = []
    for s in range(STREAMS):
        compact = ones_where((iota((PART, 256), 0) + s * PART).astype(F32) == target)
        residual = dot(compact, tokens[...]).astype(BF16)
        gathers[0, 0, s].put(residual)
        residuals.append(residual)

    own512 = pl.ds(pl.multiple_of(place.dp * 512, 512), 512)
    own256 = pl.ds(pl.multiple_of(place.dp * 256, 256), 256)
    wdo[own512, 0:128] = opening[0]
    wdo[own512, 128:256] = drive[...].astype(F32).reshape(128, 512).T.astype(BF16)
    wdo[own512, 256:384] = opening[1]
    wg[own256, :] = glu[...].astype(F32).reshape(128, 256).T.astype(BF16)
    for layer in range(2):
        wm[layer, own256, :] = merge[layer]
        we[layer, own512, :] = leaving[layer]
    counts[place.dp] = jnp.broadcast_to(jnp.sum(lens, axis=1, keepdims=True), (8, 128))

    pl.semaphore_wait(barrier, len(peers))
    for s in range(STREAMS):
        gathers[0, 0, s].start()
    for piece in range(PIECES):
        weights.start(piece)
    noted = []
    for d in range(1, NDP):
        copy = remote(counts.at[place.dp], n_send.at[d - 1], n_recv.at[d - 1], place.at_dp(d))
        copy.start()
        noted.append(copy)

    def forward(layer, kind):
        for d in Z_ORDER:
            for s in range(STREAMS):
                gathers[layer, kind, s].forward(d)

    target = jnp.where(is_live_slot[0:1], dot(counted[0:8], ones_where(row < other))[0:1] - origin, -1.0)
    for s in range(STREAMS):
        pick[s] = ones_where((iota((PART, 256), 0) + s * PART).astype(F32) == target)
    size = dot_nt(ones_where(iota((256, 32), 1) == jnp.bitwise_and(iota((256, 32), 0), 31)), lens_rows)
    number = dot_nt(ones_where(other < row), counted) - origin
    target = jnp.where(lax.shift_right_logical(row, 5).astype(F32) < size, number, -1.0)
    for s in range(STREAMS):
        spread_slot[s] = ones_where((iota((256, PART), 1) + s * PART).astype(F32) == target[:, 0:PART])
        live_slot[s] = ones_where((target >= s * PART) & (target < (s + 1) * PART), F32)
    forward(0, 0)
    size = dot_nt(ones_where(iota((256, 32), 1) == lax.shift_right_logical(iota((256, 32), 0), 3)), lens_rows)
    rank = jnp.bitwise_and(row, 7) * 32 + lax.shift_right_logical(row, 3)
    number = dot_nt(ones_where(other < rank), counted) - origin
    target = jnp.where(jnp.bitwise_and(row, 7).astype(F32) < size, number, -1.0)[:, 0:128]
    for s in range(STREAMS):
        spread_seq[s] = ones_where((iota((256, PART), 1) + s * PART).astype(F32) == target[:, 0:PART])
    live_seq[...] = ones_where((target >= 0.0) & (target < ROWS), F32)

    spread64 = ones_where(iota((64, 256), 0) == jnp.bitwise_and(iota((64, 256), 1), 63), F32)
    spread2 = ones_where(iota((64, 128), 0) == jnp.bitwise_and(iota((64, 128), 1), 63), F32)
    group4 = iota((4, 256), 0) == lax.shift_right_logical(iota((4, 256), 1), 6)
    in_group = lax.shift_right_logical(iota((64, 256), 0), 4) == lax.shift_right_logical(iota((64, 256), 1), 6)
    size_all = dot(step[...], ones_where(group4, F32), precision=HIGH)
    skip_all = dot(skip[...], spread2, precision=HIGH)
    for layer in range(2):
        rate = dot(decay[layer], spread64, precision=HIGH)
        rate = jnp.sum(jnp.where(group4, rate, 0.0), axis=0, keepdims=True)
        turning = dot(turn[layer], spread64, precision=HIGH)
        turning = jnp.sum(jnp.where(group4, turning, 0.0), axis=0, keepdims=True)
        length = size_all[layer : layer + 1]
        real = -rate
        magnitude = jnp.exp(length * real)
        decay_real = magnitude * jnp.cos(length * turning)
        decay_imag = magnitude * jnp.sin(length * turning)
        divisor = real * real + turning * turning
        params[layer, 0:1, :] = decay_real
        params[layer, 1:2, :] = decay_imag
        params[layer, 2:3, :] = ((decay_real - 1.0) * real + decay_imag * turning) / divisor
        params[layer, 3:4, :] = (decay_imag * real - (decay_real - 1.0) * turning) / divisor
        params[layer, 4:5, 0:128] = skip_all[layer : layer + 1]
        for part in range(2):
            lanes = slice(part * 256, part * 256 + 256)
            wide = jnp.where(in_group, dot(s_in[layer, part], spread64, precision=HIGH), 0.0)
            high = wide.astype(BF16)
            low = (wide - high.astype(F32)).astype(BF16)
            for k in range(2):
                inject[layer, k * 64 : k * 64 + 64, lanes] = high
                inject[layer, 128 + k * 64 : 192 + k * 64, lanes] = low
            wide = jnp.where(in_group, dot(s_out[layer, part], spread64, precision=HIGH), 0.0)
            wide = (wide if part == 0 else -wide).astype(BF16)
            readout_w[layer, 0:64, lanes] = wide
            readout_w[layer, 64:128, lanes] = wide
    weights.forward(0)

    lane = iota((PART, 128), 1)
    lane_half = iota((half, 128), 1)
    low256 = iota((256, 128), 1) < 64

    def build_gp():
        zero = jnp.zeros((256, 128), BF16)
        for k in range(8):
            plain = wg[k * 256 : k * 256 + 256, :]
            turned = swap_halves(plain.astype(F32)).astype(BF16)
            for layer in range(2):
                first, second = (plain, turned) if layer == 0 else (turned, plain)
                top = jnp.where(low256, first, zero).reshape(4, 64, 128)
                bottom = jnp.where(low256, zero, second).reshape(4, 64, 128)
                gp[layer, k * 512 : k * 512 + 512, :] = jnp.concatenate([top, bottom], axis=1).reshape(512, 128)

    def build_mp(layer):
        zero = jnp.zeros((4, 64, 128), BF16)
        for k in range(8):
            plain = wm[layer, k * 256 : k * 256 + 256, :].reshape(4, 64, 128)
            mp[layer, k * 512 : k * 512 + 512, 0:128] = jnp.concatenate([plain, zero], axis=1).reshape(512, 128)
            mp[layer, k * 512 : k * 512 + 512, 128:256] = jnp.concatenate([zero, plain], axis=1).reshape(512, 128)

    def project(buf, weight):
        total = None
        for k in range(NZ):
            term = dot(buf[k], weight(k * 512, 512))
            total = term if total is None else total + term
        return total

    gates, branches = {}, {}

    def enter(layer, s, buf):
        squares = None
        for k in range(NZ):
            value = buf[k].astype(F32)
            term = jnp.sum(value * value, axis=1, keepdims=True)
            squares = term if squares is None else squares + term
        inverse = lax.rsqrt(squares / (NZ * 512.0) + EPS)
        total = None
        for k in range(NZ):
            gain = gains[layer : layer + 1, k * 512 : k * 512 + 512]
            normed = (buf[k].astype(F32) * inverse * gain).astype(BF16)
            term = dot(normed, wdo[k * 512 : k * 512 + 512, layer * 128 : layer * 128 + 256])
            total = term if total is None else total + term
        lanes_open = slice(0, 128) if layer == 0 else slice(128, 256)
        lanes_drive = slice(128, 256) if layer == 0 else slice(0, 128)
        gates[s] = jax.nn.sigmoid(total[:, lanes_open])
        both = total[:, lanes_drive]
        mine = lane < 64 if layer == 0 else lane >= 64
        drives = jnp.where(mine, both, swap_halves(both))
        high = drives.astype(BF16).astype(F32)
        split = jnp.where(lane < 64, high, drives - high).astype(BF16)
        spread = dot(spread_slot[s], split).astype(BF16)
        moved = dot(jnp.concatenate([spread, spread], axis=1), inject[layer])
        hold_real, hold_imag = params[layer, 2:3, :], params[layer, 3:4, :]
        pushed[:, 0:256] = hold_real * moved[:, 0:256] - hold_imag * moved[:, 256:512]
        pushed[:, 256:512] = hold_real * moved[:, 256:512] + hold_imag * moved[:, 0:256]
        decay_real = jnp.broadcast_to(params[layer, 0:1, :], (32, 256))
        decay_imag = jnp.broadcast_to(params[layer, 1:2, :], (32, 256))
        before = carried if s == 0 else out_state
        state_real, state_imag = before[layer, 0], before[layer, 1]
        for t in range(8):
            now = slice(t * 32, t * 32 + 32)
            alive = live_slot[s, now, :] > 0.5
            next_real = decay_real * state_real - decay_imag * state_imag + pushed[now, 0:256]
            next_imag = decay_real * state_imag + decay_imag * state_real + pushed[now, 256:512]
            state_real = jnp.where(alive, next_real, state_real)
            state_imag = jnp.where(alive, next_imag, state_imag)
            trail[now, 0:256] = state_real.astype(BF16)
            trail[now, 256:512] = state_imag.astype(BF16)
        out_state[layer, 0] = state_real
        out_state[layer, 1] = state_imag
        chosen = dot(pick[s], trail[...]).astype(BF16)
        readout = dot_nt(chosen, readout_w[layer]) + params[layer, 4:5, 0:128] * drives
        inner = math.sqrt(2.0 / math.pi) * (readout + 0.044715 * (readout * readout * readout))
        activated = (readout * (0.5 * (1.0 + jnp.tanh(inner)))).astype(BF16).astype(F32)
        packed = jnp.where(lane_half < 64, activated[0:half], activated[half:PART])
        branches[s] = packed
        return packed.astype(BF16)

    def switch(layer, s, buf):
        gating = project(buf, lambda k, n: gp[layer, k : k + n, :])
        return (branches[s] * jax.nn.sigmoid(gating)).astype(BF16)

    def join(layer, s, buf):
        merged = project(buf, lambda k, n: mp[layer, k : k + n, :])
        merged = jnp.concatenate([merged[:, 0:128], merged[:, 128:256]], axis=0)
        return (gates[s] * merged).astype(BF16)

    def leave(layer, s, buf):
        branch = project(buf, lambda k, n: we[layer, k : k + n, :])
        residuals[s] = (residuals[s].astype(F32) + branch).astype(BF16)
        return residuals[s]

    def ready(layer, kind):
        if kind == 0:
            weights.finish(4 * layer)
        elif kind == 1 and layer == 0:
            weights.finish(1)
            build_gp()
        elif kind == 2:
            weights.finish(2 + 3 * layer)
            build_mp(layer)
        elif kind == 3:
            weights.finish(3 + 3 * layer)

    relays = {(0, 0): (1, 2), (0, 1): (3, 4), (0, 2): (5,), (0, 3): (6,)}
    for layer in range(2):
        for kind, compute in enumerate((enter, switch, join, leave)):
            ready(layer, kind)
            following = (layer, kind + 1) if kind < 3 else (layer + 1, 0)
            for s in range(STREAMS):
                done = gathers[layer, kind, s]
                done.finish()
                value = compute(layer, s, done.buf)
                if following[0] < 2:
                    gathers[following + (s,)].put(value)
                    gathers[following + (s,)].start()
            if following[0] < 2:
                forward(*following)
            for piece in relays.get((layer, kind), ()):
                weights.forward(piece)

    spread = None
    for s in range(STREAMS):
        term = dot(spread_seq[s], residuals[s])
        spread = term if spread is None else spread + term
    out_tokens[...] = jnp.where(live_seq[...] > 0.5, spread.astype(BF16), tokens[...])
    for d in range(1, NDP):
        theirs = counts.at[(place.dp + NDP - d) % NDP]
        remote(theirs, n_send.at[d - 1], n_recv.at[d - 1], place.at_dp(d)).wait_recv()
    out_count[...] = jnp.max(counts[...], axis=0)
    for copy in noted:
        copy.wait_send()
    weights.drain()


def layers(number):
    vmem = pl.BlockSpec(memory_space=pltpu.VMEM)
    half = PART // 2
    gather_count = 8 * STREAMS
    return pl.pallas_call(
        kernel,
        name="layers",
        out_shape=(
            jax.ShapeDtypeStruct((256, 128), BF16),
            jax.ShapeDtypeStruct((2, 2, 32, 256), F32),
            jax.ShapeDtypeStruct((8, 128), F32),
        ),
        in_specs=[vmem] * 16,
        out_specs=(vmem, vmem, vmem),
        scratch_shapes=[
            pltpu.VMEM((4096, 384), BF16),
            pltpu.VMEM((2048, 128), BF16),
            pltpu.VMEM((2, 2048, 128), BF16),
            pltpu.VMEM((2, 4096, 128), BF16),
            pltpu.VMEM((2, 4096, 128), BF16),
            pltpu.VMEM((2, 4096, 256), BF16),
            pltpu.VMEM((2, 2, STREAMS, NZ, PART, 512), BF16),
            pltpu.VMEM((2, 2, STREAMS, NZ, half, 512), BF16),
            pltpu.VMEM((STREAMS, PART, 256), BF16),
            pltpu.VMEM((STREAMS, 256, PART), BF16),
            pltpu.VMEM((STREAMS, 256, PART), BF16),
            pltpu.VMEM((256, 128), F32),
            pltpu.VMEM((STREAMS, 256, 256), F32),
            pltpu.VMEM((2, 8, 256), F32),
            pltpu.VMEM((2, 256, 512), BF16),
            pltpu.VMEM((2, 128, 512), BF16),
            pltpu.VMEM((256, 512), F32),
            pltpu.VMEM((256, 512), BF16),
            pltpu.VMEM((NDP, 8, 128), F32),
            pltpu.SemaphoreType.DMA((PIECES, 3)),
            pltpu.SemaphoreType.DMA((PIECES, 3)),
            pltpu.SemaphoreType.DMA((PIECES, 4)),
            pltpu.SemaphoreType.DMA((PIECES, 4)),
            pltpu.SemaphoreType.DMA((gather_count, 31)),
            pltpu.SemaphoreType.DMA((gather_count, 31)),
            pltpu.SemaphoreType.DMA((NDP - 1,)),
            pltpu.SemaphoreType.DMA((NDP - 1,)),
        ],
        compiler_params=pltpu.CompilerParams(
            collective_id=number, has_side_effects=True, vmem_limit_bytes=60 * 1024 * 1024
        ),
    )


def shards(tokens, lengths, norm_gains, drive, opening, glu, merge, leaving, decay, turn, step, s_in, s_out, skip, carried):
    lengths = lengths.reshape(1, 32)
    rest = (
        norm_gains,
        drive.swapaxes(1, 2),
        opening,
        glu.swapaxes(1, 2),
        merge,
        leaving,
        decay,
        turn,
        step,
        s_in.swapaxes(3, 4).reshape(2, 2, 64, 64),
        s_out.reshape(2, 2, 64, 64),
        skip,
    )

    def some(number, start, tokens, state):
        return layers(number)(tokens, lengths, jnp.full((1, 1), start, F32), *rest, state)

    updated, state, count = some(0, 0.0, tokens.reshape(256, 128), carried)
    updated, state = lax.cond(
        count[0, 0] > ROWS,
        lambda tokens, state: some(1, float(ROWS), tokens, state)[0:2],
        lambda tokens, state: (tokens, state),
        updated,
        state,
    )
    return updated.reshape(32, 8, 128), state


def solution(mesh):
    placed = (
        P("dp", None, "tp"),
        P("dp"),
        P(),
        P(None, "dp", "tp"),
        P(None, "dp", "tp"),
        P(None, "dp", "tp"),
        P(None, "dp", "tp"),
        P(None, "dp", "tp"),
        P(None, "tp", None),
        P(None, "tp", None),
        P(None, "tp"),
        P(None, None, "tp", None, None),
        P(None, None, "tp", None, None),
        P(None, "tp"),
        P(None, None, "dp", "tp"),
    )
    return jax.shard_map(
        shards,
        mesh=mesh,
        in_specs=placed,
        out_specs=(P("dp", None, "tp"), P(None, None, "dp", "tp")),
        check_vma=False,
    )
```

time: 199 us -> 129 us (0.65)
  Pallas kernels: 191 us -> 123 us
  local copies, waits for them, and re-layouts: 5.71 us -> 3.21 us
    pallas_call x1, Pallas kernels: 191 us -> 123 us  [some(): layers(number)(tokens, lengths, jnp.full((1, 1), start, F32), *rest, state)]
    unnamed x11 -> x28, local copies, waits for them, and re-layouts: 5.71 us -> 2.02 us
where the time goes in v2:
time: 129 us; the launch traced here: 128 us
  Pallas kernels  123 us (95%)
  local copies, waits for them, and re-layouts  3.21 us (2%)
  between operations  1.45 us (1%)
    pallas_call x1, Pallas kernels, some(): layers(number)(tokens, lengths, jnp.full((1, 1), start, F32), *rest, state)  123 us

profile of v2, /device:TPU:32, one launch (start us, length us, event | category | flops | bytes accessed | tf_op | source)
XLA Modules:
  0.0 127.9 jit_solution(6821117561364552529)
XLA Ops:
  0.6 0.0 copy-start.11
  0.6 0.0 copy-start.12
  0.7 0.0 copy-start.9
  0.7 0.0 copy-start.8
  0.7 0.0 copy-start.10
  0.7 0.6 copy-done.11
  1.3 0.0 copy-done.12
  1.3 0.0 copy-done.9
  1.4 0.0 copy-done.8
  1.4 0.0 copy-done.10
  1.4 0.0 copy-start
  1.4 0.0 copy-start.1
  1.4 0.0 copy-start.2
  1.4 0.0 copy-start.3
  1.4 0.0 copy-start.4
  1.4 0.0 copy-start.5
  1.4 0.0 copy-start.6
  1.4 0.0 copy-start.7
  1.4 123.1 %layers.3 = (bf16[256,128]{1,0:T(8,128)(2,1)S(1)}, f32[2,2,32,256]{3,2,1,0:T(8,128)S(1)}, f32[8,128]{1,0:T(8,128)}) custom-call(bf16[256,128]{1,0:T(8,128)(2,1)} %bitcast.19, s32[1,32]{1,0:T(1,128)S(1)} %bitcast.20, f32[1,1]{1,0:T(1,128)} %constant.2.clone.1.base, f32[2,4096]{1,0:T(2,128)} %gains.1, bf16[2,64,512]{2,1,0:T(8,128)(2,1)} %bitcast.10, ...), custom_call_target="tpu_custom_call" | custom-call | tf_op jit(solution)/shard_map/layers/pallas_call | solution.py:546
  124.5 1.2 slice.3
  126.4 0.0 copy-done
  126.4 0.0 copy-done.1
  126.4 0.0 copy-done.2
  126.4 0.0 copy-done.3
  126.4 0.0 copy-done.4
  126.4 0.0 copy-done.5
  126.4 0.0 copy-done.6
  126.4 0.0 copy-done.7
  126.5 0.2 conditional.1
  126.7 0.6 copy.25
  127.3 0.7 copy.26
Async XLA Ops:
  0.6 0.7 copy-start.11
  0.6 0.7 copy-start.12
  0.7 0.7 copy-start.9
  0.7 0.7 copy-start.8
  0.7 0.7 copy-start.10
  1.4 125.0 %copy-start = (bf16[2,512,128]{2,1,0:T(8,128)(2,1)S(1)}, bf16[2,512,128]{2,1,0:T(8,128)(2,1)}, u32[]{:S(2)}) copy-start(bf16[2,512,128]{2,1,0:T(8,128)(2,1)} %opening.1) | copy-start | bytes 786436
  1.4 125.0 %copy-start.1 = (bf16[2,512,128]{2,1,0:T(8,128)(2,1)S(1)}, bf16[2,512,128]{2,1,0:T(8,128)(2,1)}, u32[]{:S(2)}) copy-start(bf16[2,512,128]{2,1,0:T(8,128)(2,1)} %leaving.1) | copy-start | bytes 786436
  1.4 125.0 %copy-start.2 = (bf16[2,512,64]{1,2,0:T(8,128)(2,1)S(1)}, bf16[2,512,64]{1,2,0:T(8,128)(2,1)}, u32[]{:S(2)}) copy-start(bf16[2,512,64]{1,2,0:T(8,128)(2,1)} %param.20) | copy-start | bytes 393220
  1.4 125.0 %copy-start.3 = (bf16[2,256,128]{2,1,0:T(8,128)(2,1)S(1)}, bf16[2,256,128]{2,1,0:T(8,128)(2,1)}, u32[]{:S(2)}) copy-start(bf16[2,256,128]{2,1,0:T(8,128)(2,1)} %merge.1) | copy-start | bytes 393220
  1.4 125.0 %copy-start.4 = (f32[2,2,4,64,16]{3,4,2,1,0:T(8,128)S(1)}, f32[2,2,4,64,16]{3,4,2,1,0:T(8,128)}, u32[]{:S(2)}) copy-start(f32[2,2,4,64,16]{3,4,2,1,0:T(8,128)} %param.28) | copy-start | bytes 196612
  1.4 125.0 %copy-start.5 = (f32[2,2,4,16,64]{4,3,2,1,0:T(8,128)S(1)}, f32[2,2,4,16,64]{4,3,2,1,0:T(8,128)}, u32[]{:S(2)}) copy-start(f32[2,2,4,16,64]{4,3,2,1,0:T(8,128)} %param.29) | copy-start | bytes 196612
  1.4 125.0 %copy-start.6 = (bf16[2,256,64]{1,2,0:T(8,128)(2,1)S(1)}, bf16[2,256,64]{1,2,0:T(8,128)(2,1)}, u32[]{:S(2)}) copy-start(bf16[2,256,64]{1,2,0:T(8,128)(2,1)} %param.22) | copy-start | bytes 196612
  1.4 125.0 %copy-start.7 = (f32[2,4096]{1,0:T(2,128)S(1)}, f32[2,4096]{1,0:T(2,128)}, u32[]{:S(2)}) copy-start(f32[2,4096]{1,0:T(2,128)} %gains.1) | copy-start | bytes 98308

commit v3 on v2

--- a/solution.py
+++ b/solution.py
@@ -1,3 +1,4 @@
+import functools
 import math
 
 import jax
@@ -12,7 +13,7 @@
 EPS = 1e-05
 NZ, NX, NY, NDP = 8, 4, 4, 8
 Z_ORDER, X_ORDER = (1, 7, 2, 6, 3, 5, 4), (1, 3, 2)
-ROWS, STREAMS = 128, 1
+ROWS, STREAMS = 128, 2
 PART = ROWS // STREAMS
 LANES = 128
 F32, BF16 = jnp.float32, jnp.bfloat16
@@ -72,59 +73,48 @@
 class Gather:
     def __init__(self, place, buf, send, recv):
         self.p, self.buf, self.send, self.recv = place, buf, send, recv
-        self.sent = []
 
     def block(self, dz, dx):
         lanes = pl.ds(pl.multiple_of((self.p.x + dx) % NX * LANES, LANES), LANES)
         return self.buf.at[(self.p.z + dz) % NZ, :, lanes]
 
-    def go(self, ref, index, device):
-        copy = remote(ref, self.send.at[index], self.recv.at[index], device)
-        copy.start()
-        self.sent.append(copy)
-
-    def arrive(self, ref, index):
-        remote(ref, self.send.at[index], self.recv.at[index], self.p.partner()).wait_recv()
-
     def put(self, value):
         lanes = pl.ds(pl.multiple_of(self.p.x * LANES, LANES), LANES)
         self.buf[self.p.z, :, lanes] = value
 
+    def along_x(self, ref):
+        for e in X_ORDER:
+            remote(ref, self.send.at[1], self.recv.at[7], self.p.at_x(e)).start()
+
     def start(self):
         for d in Z_ORDER:
-            self.go(self.block(0, 0), d - 1, self.p.at_z(d))
-        for e in X_ORDER:
-            self.go(self.block(0, 0), 6 + e, self.p.at_x(e))
+            remote(self.block(0, 0), self.send.at[0], self.recv.at[d - 1], self.p.at_z(d)).start()
+        self.along_x(self.block(0, 0))
 
     def forward(self, d):
         ref = self.block(NZ - d, 0)
-        self.arrive(ref, d - 1)
-        for e in X_ORDER:
-            self.go(ref, 6 + d * 3 + e, self.p.at_x(e))
+        remote(ref, self.send.at[0], self.recv.at[d - 1], self.p.partner()).wait_recv()
+        self.along_x(ref)
 
     def finish(self):
-        for e in X_ORDER:
-            self.arrive(self.block(0, NX - e), 6 + e)
-        for d in Z_ORDER:
-            for e in X_ORDER:
-                self.arrive(self.block(NZ - d, NX - e), 6 + d * 3 + e)
-        for copy in self.sent:
-            copy.wait_send()
+        seven, most = self.buf.at[pl.ds(0, 7), :, pl.ds(0, 128)], self.buf.at[:, :, pl.ds(0, 384)]
+        remote(most, self.send.at[1], self.recv.at[7], self.p.partner()).wait_recv()
+        remote(seven, self.send.at[0], self.recv.at[0], self.p.partner()).wait_send()
+        remote(most, self.send.at[1], self.recv.at[7], self.p.partner()).wait_send()
 
 
 class Weights:
-    def __init__(self, place, wdo, wg, wm, we, y_send, y_recv, c_send, c_recv):
+    def __init__(self, place, wdo, wg, wm, we, send, recv):
         self.p = place
         self.refs = (wdo, wg, wm, we)
-        self.sems = (y_send, y_recv, c_send, c_recv)
-        self.sent = []
-
-    def region(self, piece, shard):
+        self.send, self.recv = send, recv
+
+    def region(self, piece, shard, count=1):
         wdo, wg, wm, we = self.refs
         if piece in (0, 3, 4, 6):
-            rows = pl.ds(pl.multiple_of(shard * 512, 512), 512)
+            rows = pl.ds(pl.multiple_of(shard * 512, 512), 512 * count)
         else:
-            rows = pl.ds(pl.multiple_of(shard * 256, 256), 256)
+            rows = pl.ds(pl.multiple_of(shard * 256, 256), 256 * count)
         if piece == 0:
             return wdo.at[rows, pl.ds(0, 256)]
         if piece == 4:
@@ -142,47 +132,57 @@
         return (self.p.y + step) % NY * 2 + 1 - self.p.core
 
     def y_copy(self, piece, d, shard):
-        y_send, y_recv, _, _ = self.sems
-        return remote(self.region(piece, shard), y_send.at[piece, d - 1], y_recv.at[piece, d - 1], self.p.at_y(d))
-
-    def c_copy(self, piece, d, shard):
-        _, _, c_send, c_recv = self.sems
-        return remote(self.region(piece, shard), c_send.at[piece, d], c_recv.at[piece, d], self.p.partner())
-
-    def begin(self, copy):
-        copy.start()
-        self.sent.append(copy)
+        ref = self.region(piece, shard)
+        return remote(ref, self.send.at[piece], self.recv.at[piece, d - 1], self.p.at_y(d))
+
+    def c_copy(self, piece, shard, count=1):
+        ref = self.region(piece, shard, count)
+        return remote(ref, self.send.at[piece], self.recv.at[piece, 3], self.p.partner())
 
     def start(self, piece):
         for d in (1, 3, 2):
-            self.begin(self.y_copy(piece, d, self.p.dp))
-        self.begin(self.c_copy(piece, 0, self.p.dp))
+            self.y_copy(piece, d, self.p.dp).start()
+        self.c_copy(piece, self.p.dp).start()
 
     def forward(self, piece):
         for d in (1, 3, 2):
-            shard = self.like(NY - d)
+            shard = (self.p.y + NY - d) % NY * 2 + self.p.core
             self.y_copy(piece, d, shard).wait_recv()
-            self.begin(self.c_copy(piece, d, shard))
+            self.c_copy(piece, shard).start()
 
     def finish(self, piece):
-        for d in range(NY):
-            self.c_copy(piece, d, self.unlike((NY - d) % NY)).wait_recv()
+        self.c_copy(piece, 0, 4).wait_recv()
 
     def drain(self):
-        for copy in self.sent:
-            copy.wait_send()
+        for piece in range(PIECES):
+            self.c_copy(piece, 0, 7).wait_send()
 
 
 def kernel(
+    origin,
+    tokens_h,
+    lengths_h,
+    gains_h,
+    drive_h,
+    opening_h,
+    glu_h,
+    merge_h,
+    leaving_h,
+    decay_h,
+    turn_h,
+    step_h,
+    s_in_h,
+    s_out_h,
+    skip_h,
+    carried_h,
+    out_tokens_h,
+    out_state_h,
+    out_count_h,
     tokens,
     lengths,
-    base,
     gains,
     drive,
-    opening,
     glu,
-    merge,
-    leaving,
     decay,
     turn,
     step,
@@ -212,16 +212,44 @@
     pushed,
     trail,
     counts,
-    y_send,
-    y_recv,
-    c_send,
-    c_recv,
+    w_send,
+    w_recv,
     g_send,
     g_recv,
-    n_send,
-    n_recv,
+    n_sem,
+    l_sem,
 ):
     place = Place()
+    own512 = pl.ds(pl.multiple_of(place.dp * 512, 512), 512)
+    own256 = pl.ds(pl.multiple_of(place.dp * 256, 256), 256)
+    local = {}
+    for name, source, target in (
+        ("tokens", tokens_h, tokens),
+        ("lengths", lengths_h, lengths),
+        ("open0", opening_h.at[0], wdo.at[own512, pl.ds(0, 128)]),
+        ("drive", drive_h, drive),
+        ("glu", glu_h, glu),
+        ("merge0", merge_h.at[0], wm.at[0, own256, :]),
+        ("exit0", leaving_h.at[0], we.at[0, own512, :]),
+        ("open1", opening_h.at[1], wdo.at[own512, pl.ds(256, 128)]),
+        ("merge1", merge_h.at[1], wm.at[1, own256, :]),
+        ("exit1", leaving_h.at[1], we.at[1, own512, :]),
+        ("decay", decay_h, decay),
+        ("turn", turn_h, turn),
+        ("step", step_h, step),
+        ("s_in", s_in_h, s_in),
+        ("s_out", s_out_h, s_out),
+        ("skip", skip_h, skip),
+        ("gains", gains_h, gains),
+        ("carried", carried_h, carried),
+        ("out0", out_state.at[0], out_state_h.at[0]),
+        ("out1", out_state.at[1], out_state_h.at[1]),
+        ("out_tokens", out_tokens, out_tokens_h),
+        ("out_count", out_count, out_count_h),
+    ):
+        local[name] = pltpu.make_async_copy(source, target, l_sem.at[len(local)])
+        if not name.startswith("out"):
+            local[name].start()
     half = PART // 2
     barrier = pltpu.get_barrier_semaphore()
     peers = [place.at_x(d) for d in range(1, NX)] + [place.at_z(d) for d in range(1, NZ)]
@@ -236,8 +264,9 @@
                 ref = (gx.at[layer, kind // 3, s]) if kind in (0, 3) else ga.at[layer, kind - 1, s]
                 index = (layer * 4 + kind) * STREAMS + s
                 gathers[layer, kind, s] = Gather(place, ref, g_send.at[index], g_recv.at[index])
-    weights = Weights(place, wdo, wg, wm, we, y_send, y_recv, c_send, c_recv)
-
+    weights = Weights(place, wdo, wg, wm, we, w_send, w_recv)
+
+    local["lengths"].wait()
     lens = lengths[...].astype(F32)
     lens_rows = jnp.broadcast_to(lens, (256, 32)).astype(BF16)
     seq, col = iota((32, 256), 0), iota((32, 256), 1)
@@ -249,40 +278,36 @@
     is_live_seq = jnp.bitwise_and(iota((1, 256), 1), 7).astype(F32) < size_seq
     rank_seq = jnp.bitwise_and(other, 7) * 32 + lax.shift_right_logical(other, 3)
     number_seq = dot(counted[0:8], ones_where(row < rank_seq))[0:1]
-    origin = base[...]
     target = jnp.where(is_live_seq, number_seq - origin, -1.0)
     residuals = []
+    local["tokens"].wait()
     for s in range(STREAMS):
         compact = ones_where((iota((PART, 256), 0) + s * PART).astype(F32) == target)
         residual = dot(compact, tokens[...]).astype(BF16)
         gathers[0, 0, s].put(residual)
         residuals.append(residual)
 
-    own512 = pl.ds(pl.multiple_of(place.dp * 512, 512), 512)
-    own256 = pl.ds(pl.multiple_of(place.dp * 256, 256), 256)
-    wdo[own512, 0:128] = opening[0]
-    wdo[own512, 128:256] = drive[...].astype(F32).reshape(128, 512).T.astype(BF16)
-    wdo[own512, 256:384] = opening[1]
-    wg[own256, :] = glu[...].astype(F32).reshape(128, 256).T.astype(BF16)
-    for layer in range(2):
-        wm[layer, own256, :] = merge[layer]
-        we[layer, own512, :] = leaving[layer]
     counts[place.dp] = jnp.broadcast_to(jnp.sum(lens, axis=1, keepdims=True), (8, 128))
 
     pl.semaphore_wait(barrier, len(peers))
     for s in range(STREAMS):
         gathers[0, 0, s].start()
-    for piece in range(PIECES):
-        weights.start(piece)
-    noted = []
+    local["drive"].wait()
+    wdo[own512, 128:256] = drive[...].astype(F32).reshape(128, 512).T.astype(BF16)
+    local["open0"].wait()
+    weights.start(0)
+    local["glu"].wait()
+    wg[own256, :] = glu[...].astype(F32).reshape(128, 256).T.astype(BF16)
+    weights.start(1)
+    for piece, name in enumerate(("merge0", "exit0", "open1", "merge1", "exit1")):
+        local[name].wait()
+        weights.start(piece + 2)
     for d in range(1, NDP):
-        copy = remote(counts.at[place.dp], n_send.at[d - 1], n_recv.at[d - 1], place.at_dp(d))
-        copy.start()
-        noted.append(copy)
+        remote(counts.at[place.dp], n_sem.at[0], n_sem.at[1], place.at_dp(d)).start()
 
     def forward(layer, kind):
-        for d in Z_ORDER:
-            for s in range(STREAMS):
+        for s in range(STREAMS):
+            for d in Z_ORDER:
                 gathers[layer, kind, s].forward(d)
 
     target = jnp.where(is_live_slot[0:1], dot(counted[0:8], ones_where(row < other))[0:1] - origin, -1.0)
@@ -303,6 +328,8 @@
         spread_seq[s] = ones_where((iota((256, PART), 1) + s * PART).astype(F32) == target[:, 0:PART])
     live_seq[...] = ones_where((target >= 0.0) & (target < ROWS), F32)
 
+    for name in ("decay", "turn", "step", "s_in", "s_out", "skip", "gains", "carried"):
+        local[name].wait()
     spread64 = ones_where(iota((64, 256), 0) == jnp.bitwise_and(iota((64, 256), 1), 63), F32)
     spread2 = ones_where(iota((64, 128), 0) == jnp.bitwise_and(iota((64, 128), 1), 63), F32)
     group4 = iota((4, 256), 0) == lax.shift_right_logical(iota((4, 256), 1), 6)
@@ -459,6 +486,8 @@
                     gathers[following + (s,)].start()
             if following[0] < 2:
                 forward(*following)
+            if kind == 0:
+                local[f"out{layer}"].start()
             for piece in relays.get((layer, kind), ()):
                 weights.forward(piece)
 
@@ -467,30 +496,47 @@
         term = dot(spread_seq[s], residuals[s])
         spread = term if spread is None else spread + term
     out_tokens[...] = jnp.where(live_seq[...] > 0.5, spread.astype(BF16), tokens[...])
-    for d in range(1, NDP):
-        theirs = counts.at[(place.dp + NDP - d) % NDP]
-        remote(theirs, n_send.at[d - 1], n_recv.at[d - 1], place.at_dp(d)).wait_recv()
+    local["out_tokens"].start()
+    theirs = remote(counts.at[pl.ds(0, NDP - 1)], n_sem.at[0], n_sem.at[1], place.partner())
+    theirs.wait_recv()
+    theirs.wait_send()
     out_count[...] = jnp.max(counts[...], axis=0)
-    for copy in noted:
-        copy.wait_send()
+    local["out_count"].start()
     weights.drain()
+    for name in ("out0", "out1", "out_tokens", "out_count"):
+        local[name].wait()
 
 
 def layers(number):
-    vmem = pl.BlockSpec(memory_space=pltpu.VMEM)
+    anywhere = pl.BlockSpec(memory_space=pl.ANY)
     half = PART // 2
     gather_count = 8 * STREAMS
     return pl.pallas_call(
-        kernel,
-        name="layers",
+        functools.partial(kernel, float(number * ROWS)),
+        name=f"layers_{number}",
         out_shape=(
             jax.ShapeDtypeStruct((256, 128), BF16),
             jax.ShapeDtypeStruct((2, 2, 32, 256), F32),
             jax.ShapeDtypeStruct((8, 128), F32),
         ),
-        in_specs=[vmem] * 16,
-        out_specs=(vmem, vmem, vmem),
+        in_specs=[anywhere] * 15,
+        out_specs=(anywhere, anywhere, anywhere),
         scratch_shapes=[
+            pltpu.VMEM((256, 128), BF16),
+            pltpu.VMEM((1, 32), jnp.int32),
+            pltpu.VMEM((2, 4096), F32),
+            pltpu.VMEM((2, 64, 512), BF16),
+            pltpu.VMEM((2, 64, 256), BF16),
+            pltpu.VMEM((2, 4, 64), F32),
+            pltpu.VMEM((2, 4, 64), F32),
+            pltpu.VMEM((2, 4), F32),
+            pltpu.VMEM((2, 2, 64, 64), F32),
+            pltpu.VMEM((2, 2, 64, 64), F32),
+            pltpu.VMEM((2, 64), F32),
+            pltpu.VMEM((2, 2, 32, 256), F32),
+            pltpu.VMEM((256, 128), BF16),
+            pltpu.VMEM((2, 2, 32, 256), F32),
+            pltpu.VMEM((8, 128), F32),
             pltpu.VMEM((4096, 384), BF16),
             pltpu.VMEM((2048, 128), BF16),
             pltpu.VMEM((2, 2048, 128), BF16),
@@ -510,14 +556,12 @@
             pltpu.VMEM((256, 512), F32),
             pltpu.VMEM((256, 512), BF16),
             pltpu.VMEM((NDP, 8, 128), F32),
-            pltpu.SemaphoreType.DMA((PIECES, 3)),
-            pltpu.SemaphoreType.DMA((PIECES, 3)),
+            pltpu.SemaphoreType.DMA((PIECES,)),
             pltpu.SemaphoreType.DMA((PIECES, 4)),
-            pltpu.SemaphoreType.DMA((PIECES, 4)),
-            pltpu.SemaphoreType.DMA((gather_count, 31)),
-            pltpu.SemaphoreType.DMA((gather_count, 31)),
-            pltpu.SemaphoreType.DMA((NDP - 1,)),
-            pltpu.SemaphoreType.DMA((NDP - 1,)),
+            pltpu.SemaphoreType.DMA((gather_count, 2)),
+            pltpu.SemaphoreType.DMA((gather_count, 8)),
+            pltpu.SemaphoreType.DMA((2,)),
+            pltpu.SemaphoreType.DMA((22,)),
         ],
         compiler_params=pltpu.CompilerParams(
             collective_id=number, has_side_effects=True, vmem_limit_bytes=60 * 1024 * 1024
@@ -542,13 +586,13 @@
         skip,
     )
 
-    def some(number, start, tokens, state):
-        return layers(number)(tokens, lengths, jnp.full((1, 1), start, F32), *rest, state)
-
-    updated, state, count = some(0, 0.0, tokens.reshape(256, 128), carried)
+    def some(number, tokens, state):
+        return layers(number)(tokens, lengths, *rest, state)
+
+    updated, state, count = some(0, tokens.reshape(256, 128), carried)
     updated, state = lax.cond(
         count[0, 0] > ROWS,
-        lambda tokens, state: some(1, float(ROWS), tokens, state)[0:2],
+        lambda tokens, state: some(1, tokens, state)[0:2],
         lambda tokens, state: (tokens, state),
         updated,
         state,

time: 129 us -> 111 us (0.86)
  Pallas kernels: 123 us -> 106 us
    pallas_call x1, Pallas kernels: 123 us -> 106 us  [some(): return layers(number)(tokens, lengths, *rest, state)]
where the time goes in v3:
time: 111 us
  Pallas kernels  106 us (95%)
  local copies, waits for them, and re-layouts  3.21 us (3%)
  between operations  1.45 us (1%)
    pallas_call x1, Pallas kernels, some(): return layers(number)(tokens, lengths, *rest, state)  106 us

profile of v3, /device:TPU:32, one launch (start us, length us, event | category | flops | bytes accessed | tf_op | source)
XLA Modules:
  0.0 110.8 jit_solution(17542476814342814983)
XLA Ops:
  0.6 0.0 copy-start.11
  0.6 0.0 copy-start.12
  0.7 0.0 copy-start.9
  0.7 0.0 copy-start.8
  0.7 0.0 copy-start.10
  0.7 0.6 copy-done.11
  1.3 0.0 copy-done.12
  1.3 0.0 copy-done.9
  1.4 0.0 copy-done.8
  1.4 0.0 copy-done.10
  1.4 0.0 copy-start
  1.4 0.0 copy-start.1
  1.4 0.0 copy-start.2
  1.4 0.0 copy-start.3
  1.4 0.0 copy-start.4
  1.4 0.0 copy-start.5
  1.4 0.0 copy-start.6
  1.4 0.0 copy-start.7
  1.4 105.8 %layers_0.1 = (bf16[256,128]{1,0:T(8,128)(2,1)S(1)}, f32[2,2,32,256]{3,2,1,0:T(8,128)S(1)}, f32[8,128]{1,0:T(8,128)}) custom-call(bf16[256,128]{1,0:T(8,128)(2,1)} %bitcast.19, s32[1,32]{1,0:T(1,128)S(1)} %bitcast.20, f32[2,4096]{1,0:T(2,128)} %gains_h.1, bf16[2,64,512]{2,1,0:T(8,128)(2,1)} %bitcast.10, bf16[2,512,128]{2,1,0:T(8,128)(2,1)} %opening_h.1, ...), custom_call_target="tpu_custom_call" | custom-call | tf_op jit(solution)/shard_map/layers_0/pallas_call | solution.py:590
  107.3 1.2 %slice.3 = f32[1,1]{1,0:T(1,128)} slice(f32[8,128]{1,0:T(8,128)} %get-tuple-element.63), slice={[0:1], [0:1]} | slice | bytes 8 | tf_op jit(solution)/shard_map/slice | solution.py:594
  109.1 0.0 copy-done
  109.1 0.0 copy-done.1
  109.1 0.0 copy-done.2
  109.2 0.0 copy-done.3
  109.2 0.0 copy-done.4
  109.2 0.0 copy-done.5
  109.2 0.0 copy-done.6
  109.2 0.0 copy-done.7
  109.2 0.3 conditional.1
  109.5 0.6 copy.25
  110.1 0.7 copy.26
Async XLA Ops:
  0.6 0.7 copy-start.11
  0.6 0.7 copy-start.12
  0.7 0.7 copy-start.9
  0.7 0.7 copy-start.8
  0.7 0.7 copy-start.10
  1.4 107.8 %copy-start = (bf16[2,512,128]{2,1,0:T(8,128)(2,1)S(1)}, bf16[2,512,128]{2,1,0:T(8,128)(2,1)}, u32[]{:S(2)}) copy-start(bf16[2,512,128]{2,1,0:T(8,128)(2,1)} %opening_h.1) | copy-start | bytes 786436
  1.4 107.8 %copy-start.1 = (bf16[2,512,128]{2,1,0:T(8,128)(2,1)S(1)}, bf16[2,512,128]{2,1,0:T(8,128)(2,1)}, u32[]{:S(2)}) copy-start(bf16[2,512,128]{2,1,0:T(8,128)(2,1)} %leaving_h.1) | copy-start | bytes 786436
  1.4 107.8 %copy-start.2 = (bf16[2,512,64]{1,2,0:T(8,128)(2,1)S(1)}, bf16[2,512,64]{1,2,0:T(8,128)(2,1)}, u32[]{:S(2)}) copy-start(bf16[2,512,64]{1,2,0:T(8,128)(2,1)} %param.20) | copy-start | bytes 393220
  1.4 107.8 %copy-start.3 = (bf16[2,256,128]{2,1,0:T(8,128)(2,1)S(1)}, bf16[2,256,128]{2,1,0:T(8,128)(2,1)}, u32[]{:S(2)}) copy-start(bf16[2,256,128]{2,1,0:T(8,128)(2,1)} %merge_h.1) | copy-start | bytes 393220
  1.4 107.8 %copy-start.4 = (f32[2,2,4,64,16]{3,4,2,1,0:T(8,128)S(1)}, f32[2,2,4,64,16]{3,4,2,1,0:T(8,128)}, u32[]{:S(2)}) copy-start(f32[2,2,4,64,16]{3,4,2,1,0:T(8,128)} %param.28) | copy-start | bytes 196612
  1.4 107.8 %copy-start.5 = (f32[2,2,4,16,64]{4,3,2,1,0:T(8,128)S(1)}, f32[2,2,4,16,64]{4,3,2,1,0:T(8,128)}, u32[]{:S(2)}) copy-start(f32[2,2,4,16,64]{4,3,2,1,0:T(8,128)} %param.29) | copy-start | bytes 196612
  1.4 107.8 %copy-start.6 = (bf16[2,256,64]{1,2,0:T(8,128)(2,1)S(1)}, bf16[2,256,64]{1,2,0:T(8,128)(2,1)}, u32[]{:S(2)}) copy-start(bf16[2,256,64]{1,2,0:T(8,128)(2,1)} %param.22) | copy-start | bytes 196612
  1.4 107.8 %copy-start.7 = (f32[2,4096]{1,0:T(2,128)S(1)}, f32[2,4096]{1,0:T(2,128)}, u32[]{:S(2)}) copy-start(f32[2,4096]{1,0:T(2,128)} %gains_h.1) | copy-start | bytes 98308

commit v4 on v3

--- a/solution.py
+++ b/solution.py
@@ -177,7 +177,7 @@
     carried_h,
     out_tokens_h,
     out_state_h,
-    out_count_h,
+    out_more,
     tokens,
     lengths,
     gains,
@@ -192,7 +192,6 @@
     carried,
     out_tokens,
     out_state,
-    out_count,
     wdo,
     wg,
     wm,
@@ -245,7 +244,6 @@
         ("out0", out_state.at[0], out_state_h.at[0]),
         ("out1", out_state.at[1], out_state_h.at[1]),
         ("out_tokens", out_tokens, out_tokens_h),
-        ("out_count", out_count, out_count_h),
     ):
         local[name] = pltpu.make_async_copy(source, target, l_sem.at[len(local)])
         if not name.startswith("out"):
@@ -262,7 +260,7 @@
         for kind in range(4):
             for s in range(STREAMS):
                 ref = (gx.at[layer, kind // 3, s]) if kind in (0, 3) else ga.at[layer, kind - 1, s]
-                index = (layer * 4 + kind) * STREAMS + s
+                index = kind % 2 * STREAMS + s
                 gathers[layer, kind, s] = Gather(place, ref, g_send.at[index], g_recv.at[index])
     weights = Weights(place, wdo, wg, wm, we, w_send, w_recv)
 
@@ -500,27 +498,26 @@
     theirs = remote(counts.at[pl.ds(0, NDP - 1)], n_sem.at[0], n_sem.at[1], place.partner())
     theirs.wait_recv()
     theirs.wait_send()
-    out_count[...] = jnp.max(counts[...], axis=0)
-    local["out_count"].start()
+    out_more[0, 0] = (jnp.max(counts[...]) > ROWS).astype(jnp.int32)
     weights.drain()
-    for name in ("out0", "out1", "out_tokens", "out_count"):
+    for name in ("out0", "out1", "out_tokens"):
         local[name].wait()
 
 
 def layers(number):
-    anywhere = pl.BlockSpec(memory_space=pl.ANY)
+    anywhere = pl.BlockSpec(memory_space=pltpu.HBM)
     half = PART // 2
-    gather_count = 8 * STREAMS
+    gather_count = 2 * STREAMS
     return pl.pallas_call(
         functools.partial(kernel, float(number * ROWS)),
         name=f"layers_{number}",
         out_shape=(
             jax.ShapeDtypeStruct((256, 128), BF16),
             jax.ShapeDtypeStruct((2, 2, 32, 256), F32),
-            jax.ShapeDtypeStruct((8, 128), F32),
+            jax.ShapeDtypeStruct((1, 1), jnp.int32),
         ),
         in_specs=[anywhere] * 15,
-        out_specs=(anywhere, anywhere, anywhere),
+        out_specs=(anywhere, anywhere, pl.BlockSpec(memory_space=pltpu.SMEM)),
         scratch_shapes=[
             pltpu.VMEM((256, 128), BF16),
             pltpu.VMEM((1, 32), jnp.int32),
@@ -536,7 +533,6 @@
             pltpu.VMEM((2, 2, 32, 256), F32),
             pltpu.VMEM((256, 128), BF16),
             pltpu.VMEM((2, 2, 32, 256), F32),
-            pltpu.VMEM((8, 128), F32),
             pltpu.VMEM((4096, 384), BF16),
             pltpu.VMEM((2048, 128), BF16),
             pltpu.VMEM((2, 2048, 128), BF16),
@@ -589,9 +585,9 @@
     def some(number, tokens, state):
         return layers(number)(tokens, lengths, *rest, state)
 
-    updated, state, count = some(0, tokens.reshape(256, 128), carried)
+    updated, state, more = some(0, tokens.reshape(256, 128), carried)
     updated, state = lax.cond(
-        count[0, 0] > ROWS,
+        more[0, 0] != 0,
         lambda tokens, state: some(1, tokens, state)[0:2],
         lambda tokens, state: (tokens, state),
         updated,

time: 111 us -> 109 us (0.982)
  local copies, waits for them, and re-layouts: 3.21 us -> 2.02 us
    slice x1 -> x0, local copies, waits for them, and re-layouts: 1.19 us -> none  [shards(): count[0, 0] > ROWS]
where the time goes in v4:
time: 109 us
  Pallas kernels  105 us (96%)
  local copies, waits for them, and re-layouts  2.02 us (2%)
  between operations  1.34 us (1%)
    pallas_call x1, Pallas kernels, some(): return layers(number)(tokens, lengths, *rest, state)  105 us

profile of v4, /device:TPU:32, one launch (start us, length us, event | category | flops | bytes accessed | tf_op | source)
XLA Modules:
  0.0 108.7 jit_solution(7356446328327110693)
XLA Ops:
  0.6 0.0 copy-start.11
  0.6 0.0 copy-start.12
  0.7 0.0 copy-start.9
  0.7 0.0 copy-start.8
  0.7 0.0 copy-start.10
  0.7 0.6 copy-done.11
  1.3 0.0 copy-done.12
  1.3 0.0 copy-done.9
  1.4 0.0 copy-done.8
  1.4 0.0 copy-done.10
  1.4 0.0 copy-start
  1.4 0.0 copy-start.1
  1.4 0.0 copy-start.2
  1.4 0.0 copy-start.3
  1.4 0.0 copy-start.4
  1.4 0.0 copy-start.5
  1.4 0.0 copy-start.6
  1.4 0.0 copy-start.7
  1.4 105.1 %layers_0.1 = (bf16[256,128]{1,0:T(8,128)(2,1)S(1)}, f32[2,2,32,256]{3,2,1,0:T(8,128)S(1)}, s32[1,1]{1,0:T(1,128)}) custom-call(bf16[256,128]{1,0:T(8,128)(2,1)} %bitcast.19, s32[1,32]{1,0:T(1,128)S(1)} %bitcast.20, f32[2,4096]{1,0:T(2,128)} %gains_h.1, bf16[2,64,512]{2,1,0:T(8,128)(2,1)} %bitcast.10, bf16[2,512,128]{2,1,0:T(8,128)(2,1)} %opening_h.1, ...), custom_call_target="tpu_custom_call" | custom-call | tf_op jit(solution)/shard_map/layers_0/pallas_call | solution.py:586
  107.1 0.0 copy-done
  107.1 0.0 copy-done.1
  107.1 0.0 copy-done.2
  107.1 0.0 copy-done.3
  107.1 0.0 copy-done.4
  107.1 0.0 copy-done.5
  107.1 0.0 copy-done.6
  107.2 0.0 copy-done.7
  107.2 0.3 conditional.1
  107.4 0.6 copy.25
  108.1 0.7 copy.26
Async XLA Ops:
  0.6 0.7 copy-start.11
  0.6 0.7 copy-start.12
  0.7 0.7 copy-start.9
  0.7 0.7 copy-start.8
  0.7 0.7 copy-start.10
  1.4 105.7 %copy-start = (bf16[2,512,128]{2,1,0:T(8,128)(2,1)S(1)}, bf16[2,512,128]{2,1,0:T(8,128)(2,1)}, u32[]{:S(2)}) copy-start(bf16[2,512,128]{2,1,0:T(8,128)(2,1)} %opening_h.1) | copy-start | bytes 786436
  1.4 105.7 %copy-start.1 = (bf16[2,512,128]{2,1,0:T(8,128)(2,1)S(1)}, bf16[2,512,128]{2,1,0:T(8,128)(2,1)}, u32[]{:S(2)}) copy-start(bf16[2,512,128]{2,1,0:T(8,128)(2,1)} %leaving_h.1) | copy-start | bytes 786436
  1.4 105.7 %copy-start.2 = (bf16[2,512,64]{1,2,0:T(8,128)(2,1)S(1)}, bf16[2,512,64]{1,2,0:T(8,128)(2,1)}, u32[]{:S(2)}) copy-start(bf16[2,512,64]{1,2,0:T(8,128)(2,1)} %param.20) | copy-start | bytes 393220
  1.4 105.7 %copy-start.3 = (bf16[2,256,128]{2,1,0:T(8,128)(2,1)S(1)}, bf16[2,256,128]{2,1,0:T(8,128)(2,1)}, u32[]{:S(2)}) copy-start(bf16[2,256,128]{2,1,0:T(8,128)(2,1)} %merge_h.1) | copy-start | bytes 393220
  1.4 105.7 %copy-start.4 = (f32[2,2,4,64,16]{3,4,2,1,0:T(8,128)S(1)}, f32[2,2,4,64,16]{3,4,2,1,0:T(8,128)}, u32[]{:S(2)}) copy-start(f32[2,2,4,64,16]{3,4,2,1,0:T(8,128)} %param.28) | copy-start | bytes 196612
  1.4 105.7 %copy-start.5 = (f32[2,2,4,16,64]{4,3,2,1,0:T(8,128)S(1)}, f32[2,2,4,16,64]{4,3,2,1,0:T(8,128)}, u32[]{:S(2)}) copy-start(f32[2,2,4,16,64]{4,3,2,1,0:T(8,128)} %param.29) | copy-start | bytes 196612
  1.4 105.7 %copy-start.6 = (bf16[2,256,64]{1,2,0:T(8,128)(2,1)S(1)}, bf16[2,256,64]{1,2,0:T(8,128)(2,1)}, u32[]{:S(2)}) copy-start(bf16[2,256,64]{1,2,0:T(8,128)(2,1)} %param.22) | copy-start | bytes 196612
  1.4 105.7 %copy-start.7 = (f32[2,4096]{1,0:T(2,128)S(1)}, f32[2,4096]{1,0:T(2,128)}, u32[]{:S(2)}) copy-start(f32[2,4096]{1,0:T(2,128)} %gains_h.1) | copy-start | bytes 98308

commit v5 on v4

--- a/solution.py
+++ b/solution.py
@@ -18,7 +18,7 @@
 LANES = 128
 F32, BF16 = jnp.float32, jnp.bfloat16
 NT = (((1,), (1,)), ((), ()))
-PIECES = 7
+PIECES = 8
 
 
 def dot(a, b, **kw):
@@ -111,19 +111,21 @@
 
     def region(self, piece, shard, count=1):
         wdo, wg, wm, we = self.refs
-        if piece in (0, 3, 4, 6):
+        if piece in (0, 4, 7):
             rows = pl.ds(pl.multiple_of(shard * 512, 512), 512 * count)
         else:
             rows = pl.ds(pl.multiple_of(shard * 256, 256), 256 * count)
         if piece == 0:
-            return wdo.at[rows, pl.ds(0, 256)]
+            return wdo.at[rows, pl.ds(128, 128)]
+        if piece == 7:
+            return wdo.at[rows, pl.ds(0, 128)]
         if piece == 4:
             return wdo.at[rows, pl.ds(256, 128)]
         if piece == 1:
             return wg.at[rows, :]
         if piece in (2, 5):
             return wm.at[(piece - 2) // 3, rows, :]
-        return we.at[(piece - 3) // 3, rows, :]
+        return we.at[(piece - 3) // 3, pl.ds(shard, count)]
 
     def like(self, step):
         return (self.p.y + step) % NY * 2 + self.p.core
@@ -200,6 +202,9 @@
     mp,
     gx,
     ga,
+    gm,
+    tx,
+    rx,
     pick,
     spread_seq,
     spread_slot,
@@ -217,10 +222,14 @@
     g_recv,
     n_sem,
     l_sem,
+    q_sem,
+    e_sem,
 ):
     place = Place()
     own512 = pl.ds(pl.multiple_of(place.dp * 512, 512), 512)
     own256 = pl.ds(pl.multiple_of(place.dp * 256, 256), 256)
+    own_lanes = pl.ds(pl.multiple_of(place.x * LANES, LANES), LANES)
+    own_rows = pl.ds(pl.multiple_of(place.x * 128, 128), 128)
     local = {}
     for name, source, target in (
         ("tokens", tokens_h, tokens),
@@ -229,10 +238,10 @@
         ("drive", drive_h, drive),
         ("glu", glu_h, glu),
         ("merge0", merge_h.at[0], wm.at[0, own256, :]),
-        ("exit0", leaving_h.at[0], we.at[0, own512, :]),
+        ("exit0", leaving_h.at[0, own_rows, :], we.at[0, place.dp, :, own_lanes]),
         ("open1", opening_h.at[1], wdo.at[own512, pl.ds(256, 128)]),
         ("merge1", merge_h.at[1], wm.at[1, own256, :]),
-        ("exit1", leaving_h.at[1], we.at[1, own512, :]),
+        ("exit1", leaving_h.at[1, own_rows, :], we.at[1, place.dp, :, own_lanes]),
         ("decay", decay_h, decay),
         ("turn", turn_h, turn),
         ("step", step_h, step),
@@ -257,10 +266,10 @@
 
     gathers = {}
     for layer in range(2):
-        for kind in range(4):
+        for kind in range(3):
             for s in range(STREAMS):
-                ref = (gx.at[layer, kind // 3, s]) if kind in (0, 3) else ga.at[layer, kind - 1, s]
-                index = kind % 2 * STREAMS + s
+                ref = gx.at[layer, s] if kind == 0 else ga.at[layer, kind - 1, s]
+                index = (layer * 3 + kind) % 2 * STREAMS + s
                 gathers[layer, kind, s] = Gather(place, ref, g_send.at[index], g_recv.at[index])
     weights = Weights(place, wdo, wg, wm, we, w_send, w_recv)
 
@@ -292,14 +301,31 @@
         gathers[0, 0, s].start()
     local["drive"].wait()
     wdo[own512, 128:256] = drive[...].astype(F32).reshape(128, 512).T.astype(BF16)
-    local["open0"].wait()
     weights.start(0)
     local["glu"].wait()
     wg[own256, :] = glu[...].astype(F32).reshape(128, 256).T.astype(BF16)
     weights.start(1)
-    for piece, name in enumerate(("merge0", "exit0", "open1", "merge1", "exit1")):
-        local[name].wait()
-        weights.start(piece + 2)
+    local["open0"].wait()
+    weights.start(7)
+    local["merge0"].wait()
+    weights.start(2)
+    for layer in range(2):
+        for e in X_ORDER:
+            rows = pl.ds(pl.multiple_of((place.x + e) % NX * 128, 128), 128)
+            pltpu.make_async_remote_copy(
+                src_ref=leaving_h.at[layer, rows, :],
+                dst_ref=we.at[layer, place.dp, :, own_lanes],
+                send_sem=q_sem.at[layer, 0],
+                recv_sem=q_sem.at[layer, 1],
+                device_id=place.at_x(e),
+                device_id_type=MESH,
+            ).start()
+
+    def quarters(layer):
+        ref = we.at[layer, place.dp, :, pl.ds(0, 384)]
+        copy = remote(ref, q_sem.at[layer, 0], q_sem.at[layer, 1], place.partner())
+        copy.wait_recv()
+        copy.wait_send()
     for d in range(1, NDP):
         remote(counts.at[place.dp], n_sem.at[0], n_sem.at[1], place.at_dp(d)).start()
 
@@ -318,6 +344,11 @@
         spread_slot[s] = ones_where((iota((256, PART), 1) + s * PART).astype(F32) == target[:, 0:PART])
         live_slot[s] = ones_where((target >= s * PART) & (target < (s + 1) * PART), F32)
     forward(0, 0)
+    quarters(0)
+    quarters(1)
+    for piece, name in enumerate(("exit0", "open1", "merge1", "exit1")):
+        local[name].wait()
+        weights.start(piece + 3)
     size = dot_nt(ones_where(iota((256, 32), 1) == lax.shift_right_logical(iota((256, 32), 0), 3)), lens_rows)
     rank = jnp.bitwise_and(row, 7) * 32 + lax.shift_right_logical(row, 3)
     number = dot_nt(ones_where(other < rank), counted) - origin
@@ -402,16 +433,13 @@
             term = jnp.sum(value * value, axis=1, keepdims=True)
             squares = term if squares is None else squares + term
         inverse = lax.rsqrt(squares / (NZ * 512.0) + EPS)
-        total = None
+        both = None
         for k in range(NZ):
             gain = gains[layer : layer + 1, k * 512 : k * 512 + 512]
             normed = (buf[k].astype(F32) * inverse * gain).astype(BF16)
-            term = dot(normed, wdo[k * 512 : k * 512 + 512, layer * 128 : layer * 128 + 256])
-            total = term if total is None else total + term
-        lanes_open = slice(0, 128) if layer == 0 else slice(128, 256)
-        lanes_drive = slice(128, 256) if layer == 0 else slice(0, 128)
-        gates[s] = jax.nn.sigmoid(total[:, lanes_open])
-        both = total[:, lanes_drive]
+            buf[k] = normed
+            term = dot(normed, wdo[k * 512 : k * 512 + 512, 128:256])
+            both = term if both is None else both + term
         mine = lane < 64 if layer == 0 else lane >= 64
         drives = jnp.where(mine, both, swap_halves(both))
         high = drives.astype(BF16).astype(F32)
@@ -444,6 +472,14 @@
         branches[s] = packed
         return packed.astype(BF16)
 
+    def open_gates(layer):
+        weights.finish(7 if layer == 0 else 4)
+        for s in range(STREAMS):
+            total = project(
+                gathers[layer, 0, s].buf, lambda k, n: wdo[k : k + n, layer * 256 : layer * 256 + 128]
+            )
+            gates[s] = jax.nn.sigmoid(total)
+
     def switch(layer, s, buf):
         gating = project(buf, lambda k, n: gp[layer, k : k + n, :])
         return (branches[s] * jax.nn.sigmoid(gating)).astype(BF16)
@@ -453,14 +489,46 @@
         merged = jnp.concatenate([merged[:, 0:128], merged[:, 128:256]], axis=0)
         return (gates[s] * merged).astype(BF16)
 
-    def leave(layer, s, buf):
-        branch = project(buf, lambda k, n: we[layer, k : k + n, :])
+    def spread_mixed(layer, s, value):
+        lanes = pl.ds(pl.multiple_of(place.z * LANES, LANES), LANES)
+        gm[layer, s, :, lanes] = value
+        for d in Z_ORDER:
+            ref = gm.at[layer, s, :, lanes]
+            remote(ref, e_sem.at[layer, s, 0], e_sem.at[layer, s, 1], place.at_z(d)).start()
+
+    def leave(layer, s):
+        ref = gm.at[layer, s, :, pl.ds(0, 896)]
+        copy = remote(ref, e_sem.at[layer, s, 0], e_sem.at[layer, s, 1], place.partner())
+        copy.wait_recv()
+        copy.wait_send()
+        partial = dot(gm[layer, s], we[layer].reshape(1024, 512)).astype(BF16)
+        for k in range(NX):
+            tx[layer, s, k] = partial[:, k * 128 : k * 128 + 128]
+        for e in X_ORDER:
+            pltpu.make_async_remote_copy(
+                src_ref=tx.at[layer, s, (place.x + e) % NX],
+                dst_ref=rx.at[layer, s, place.x],
+                send_sem=e_sem.at[layer, s, 2],
+                recv_sem=e_sem.at[layer, s, 3],
+                device_id=place.at_x(e),
+                device_id_type=MESH,
+            ).start()
+        rx[layer, s, place.x] = tx[layer, s, place.x]
+
+    def settle(layer, s):
+        ref = rx.at[layer, s, pl.ds(0, 3)]
+        copy = remote(ref, e_sem.at[layer, s, 2], e_sem.at[layer, s, 3], place.partner())
+        copy.wait_recv()
+        copy.wait_send()
+        branch = rx[layer, s, 0].astype(F32)
+        for k in range(1, NX):
+            branch = branch + rx[layer, s, k].astype(F32)
         residuals[s] = (residuals[s].astype(F32) + branch).astype(BF16)
         return residuals[s]
 
     def ready(layer, kind):
-        if kind == 0:
-            weights.finish(4 * layer)
+        if kind == 0 and layer == 0:
+            weights.finish(0)
         elif kind == 1 and layer == 0:
             weights.finish(1)
             build_gp()
@@ -470,24 +538,37 @@
         elif kind == 3:
             weights.finish(3 + 3 * layer)
 
-    relays = {(0, 0): (1, 2), (0, 1): (3, 4), (0, 2): (5,), (0, 3): (6,)}
+    relays = {(0, 0): (1, 7, 2), (0, 1): (3, 4), (0, 2): (5, 6)}
     for layer in range(2):
-        for kind, compute in enumerate((enter, switch, join, leave)):
+        for kind, compute in enumerate((enter, switch, join)):
             ready(layer, kind)
-            following = (layer, kind + 1) if kind < 3 else (layer + 1, 0)
             for s in range(STREAMS):
                 done = gathers[layer, kind, s]
                 done.finish()
                 value = compute(layer, s, done.buf)
-                if following[0] < 2:
-                    gathers[following + (s,)].put(value)
-                    gathers[following + (s,)].start()
-            if following[0] < 2:
-                forward(*following)
+                if kind < 2:
+                    gathers[layer, kind + 1, s].put(value)
+                    gathers[layer, kind + 1, s].start()
+                else:
+                    spread_mixed(layer, s, value)
+            if kind < 2:
+                forward(layer, kind + 1)
             if kind == 0:
                 local[f"out{layer}"].start()
             for piece in relays.get((layer, kind), ()):
                 weights.forward(piece)
+            if kind == 0:
+                open_gates(layer)
+        ready(layer, 3)
+        for s in range(STREAMS):
+            leave(layer, s)
+        for s in range(STREAMS):
+            value = settle(layer, s)
+            if layer == 0:
+                gathers[1, 0, s].put(value)
+                gathers[1, 0, s].start()
+        if layer == 0:
+            forward(1, 0)
 
     spread = None
     for s in range(STREAMS):
@@ -536,11 +617,14 @@
             pltpu.VMEM((4096, 384), BF16),
             pltpu.VMEM((2048, 128), BF16),
             pltpu.VMEM((2, 2048, 128), BF16),
-            pltpu.VMEM((2, 4096, 128), BF16),
+            pltpu.VMEM((2, NDP, 128, 512), BF16),
             pltpu.VMEM((2, 4096, 128), BF16),
             pltpu.VMEM((2, 4096, 256), BF16),
-            pltpu.VMEM((2, 2, STREAMS, NZ, PART, 512), BF16),
+            pltpu.VMEM((2, STREAMS, NZ, PART, 512), BF16),
             pltpu.VMEM((2, 2, STREAMS, NZ, half, 512), BF16),
+            pltpu.VMEM((2, STREAMS, PART, 1024), BF16),
+            pltpu.VMEM((2, STREAMS, NX, PART, 128), BF16),
+            pltpu.VMEM((2, STREAMS, NX, PART, 128), BF16),
             pltpu.VMEM((STREAMS, PART, 256), BF16),
             pltpu.VMEM((STREAMS, 256, PART), BF16),
             pltpu.VMEM((STREAMS, 256, PART), BF16),
@@ -557,7 +641,9 @@
             pltpu.SemaphoreType.DMA((gather_count, 2)),
             pltpu.SemaphoreType.DMA((gather_count, 8)),
             pltpu.SemaphoreType.DMA((2,)),
-            pltpu.SemaphoreType.DMA((22,)),
+            pltpu.SemaphoreType.DMA((21,)),
+            pltpu.SemaphoreType.DMA((2, 2)),
+            pltpu.SemaphoreType.DMA((2, STREAMS, 4)),
         ],
         compiler_params=pltpu.CompilerParams(
             collective_id=number, has_side_effects=True, vmem_limit_bytes=60 * 1024 * 1024

time: 109 us -> 104 us (0.954)
  the two profiles are of different devices: /device:TPU:32 before, /device:TPU:16 now
where the time goes in v5:
time: 104 us
  Pallas kernels  100 us (96%)
  local copies, waits for them, and re-layouts  2.02 us (2%)
  between operations  1.34 us (1%)
    pallas_call x1, Pallas kernels, some(): return layers(number)(tokens, lengths, *rest, state)  100 us

profile of v5, /device:TPU:16, one launch (start us, length us, event | category | flops | bytes accessed | tf_op | source)
XLA Modules:
  0.0 103.9 jit_solution(7068860190119938300)
XLA Ops:
  0.6 0.0 copy-start.11
  0.6 0.0 copy-start.12
  0.7 0.0 copy-start.9
  0.7 0.0 copy-start.8
  0.7 0.0 copy-start.10
  0.7 0.6 copy-done.11
  1.3 0.0 copy-done.12
  1.3 0.0 copy-done.9
  1.4 0.0 copy-done.8
  1.4 0.0 copy-done.10
  1.4 0.0 copy-start
  1.4 0.0 copy-start.1
  1.4 0.0 copy-start.2
  1.4 0.0 copy-start.3
  1.4 0.0 copy-start.4
  1.4 0.0 copy-start.5
  1.4 0.0 copy-start.6
  1.4 0.0 copy-start.7
  1.4 100.2 %layers_0.1 = (bf16[256,128]{1,0:T(8,128)(2,1)S(1)}, f32[2,2,32,256]{3,2,1,0:T(8,128)S(1)}, s32[1,1]{1,0:T(1,128)}) custom-call(bf16[256,128]{1,0:T(8,128)(2,1)} %bitcast.19, s32[1,32]{1,0:T(1,128)S(1)} %bitcast.20, f32[2,4096]{1,0:T(2,128)} %gains_h.1, bf16[2,64,512]{2,1,0:T(8,128)(2,1)} %bitcast.10, bf16[2,512,128]{2,1,0:T(8,128)(2,1)} %opening_h.1, ...), custom_call_target="tpu_custom_call" | custom-call | tf_op jit(solution)/shard_map/layers_0/pallas_call | solution.py:672
  102.2 0.0 copy-done
  102.2 0.0 copy-done.1
  102.2 0.0 copy-done.2
  102.2 0.0 copy-done.3
  102.3 0.0 copy-done.4
  102.3 0.0 copy-done.5
  102.3 0.0 copy-done.6
  102.3 0.0 copy-done.7
  102.3 0.3 conditional.1
  102.6 0.6 copy.25
  103.2 0.7 copy.26
Async XLA Ops:
  0.6 0.7 copy-start.11
  0.6 0.7 copy-start.12
  0.7 0.7 copy-start.9
  0.7 0.7 copy-start.8
  0.7 0.7 copy-start.10
  1.4 100.8 %copy-start = (bf16[2,512,128]{2,1,0:T(8,128)(2,1)S(1)}, bf16[2,512,128]{2,1,0:T(8,128)(2,1)}, u32[]{:S(2)}) copy-start(bf16[2,512,128]{2,1,0:T(8,128)(2,1)} %opening_h.1) | copy-start | bytes 786436
  1.4 100.8 %copy-start.1 = (bf16[2,512,128]{2,1,0:T(8,128)(2,1)S(1)}, bf16[2,512,128]{2,1,0:T(8,128)(2,1)}, u32[]{:S(2)}) copy-start(bf16[2,512,128]{2,1,0:T(8,128)(2,1)} %leaving_h.1) | copy-start | bytes 786436
  1.4 100.8 %copy-start.2 = (bf16[2,512,64]{1,2,0:T(8,128)(2,1)S(1)}, bf16[2,512,64]{1,2,0:T(8,128)(2,1)}, u32[]{:S(2)}) copy-start(bf16[2,512,64]{1,2,0:T(8,128)(2,1)} %param.20) | copy-start | bytes 393220
  1.4 100.9 %copy-start.3 = (bf16[2,256,128]{2,1,0:T(8,128)(2,1)S(1)}, bf16[2,256,128]{2,1,0:T(8,128)(2,1)}, u32[]{:S(2)}) copy-start(bf16[2,256,128]{2,1,0:T(8,128)(2,1)} %merge_h.1) | copy-start | bytes 393220
  1.4 100.9 %copy-start.4 = (f32[2,2,4,64,16]{3,4,2,1,0:T(8,128)S(1)}, f32[2,2,4,64,16]{3,4,2,1,0:T(8,128)}, u32[]{:S(2)}) copy-start(f32[2,2,4,64,16]{3,4,2,1,0:T(8,128)} %param.28) | copy-start | bytes 196612
  1.4 100.9 %copy-start.5 = (f32[2,2,4,16,64]{4,3,2,1,0:T(8,128)S(1)}, f32[2,2,4,16,64]{4,3,2,1,0:T(8,128)}, u32[]{:S(2)}) copy-start(f32[2,2,4,16,64]{4,3,2,1,0:T(8,128)} %param.29) | copy-start | bytes 196612
  1.4 100.9 %copy-start.6 = (bf16[2,256,64]{1,2,0:T(8,128)(2,1)S(1)}, bf16[2,256,64]{1,2,0:T(8,128)(2,1)}, u32[]{:S(2)}) copy-start(bf16[2,256,64]{1,2,0:T(8,128)(2,1)} %param.22) | copy-start | bytes 196612
  1.4 100.9 %copy-start.7 = (f32[2,4096]{1,0:T(2,128)S(1)}, f32[2,4096]{1,0:T(2,128)}, u32[]{:S(2)}) copy-start(f32[2,4096]{1,0:T(2,128)} %gains_h.1) | copy-start | bytes 98308

commit v6 on v5

--- a/solution.py
+++ b/solution.py
@@ -12,7 +12,7 @@
 HIGH = lax.Precision.HIGHEST
 EPS = 1e-05
 NZ, NX, NY, NDP = 8, 4, 4, 8
-Z_ORDER, X_ORDER = (1, 7, 2, 6, 3, 5, 4), (1, 3, 2)
+Z_ORDER, X_ORDER = (1, 7, 2, 6, 3, 5, 4), (2, 1, 3)
 ROWS, STREAMS = 128, 2
 PART = ROWS // STREAMS
 LANES = 128
@@ -97,8 +97,11 @@
         self.along_x(ref)
 
     def finish(self):
+        most = self.buf.at[:, :, pl.ds(0, 384)]
+        remote(most, self.send.at[1], self.recv.at[7], self.p.partner()).wait_recv()
+
+    def drain(self):
         seven, most = self.buf.at[pl.ds(0, 7), :, pl.ds(0, 128)], self.buf.at[:, :, pl.ds(0, 384)]
-        remote(most, self.send.at[1], self.recv.at[7], self.p.partner()).wait_recv()
         remote(seven, self.send.at[0], self.recv.at[0], self.p.partner()).wait_send()
         remote(most, self.send.at[1], self.recv.at[7], self.p.partner()).wait_send()
 
@@ -203,6 +206,7 @@
     gx,
     ga,
     gm,
+    nx,
     tx,
     rx,
     pick,
@@ -424,7 +428,7 @@
             total = term if total is None else total + term
         return total
 
-    gates, branches = {}, {}
+    gates, branches, waiting = {}, {}, []
 
     def enter(layer, s, buf):
         squares = None
@@ -437,7 +441,7 @@
         for k in range(NZ):
             gain = gains[layer : layer + 1, k * 512 : k * 512 + 512]
             normed = (buf[k].astype(F32) * inverse * gain).astype(BF16)
-            buf[k] = normed
+            nx[s, k] = normed
             term = dot(normed, wdo[k * 512 : k * 512 + 512, 128:256])
             both = term if both is None else both + term
         mine = lane < 64 if layer == 0 else lane >= 64
@@ -476,7 +480,7 @@
         weights.finish(7 if layer == 0 else 4)
         for s in range(STREAMS):
             total = project(
-                gathers[layer, 0, s].buf, lambda k, n: wdo[k : k + n, layer * 256 : layer * 256 + 128]
+                nx.at[s], lambda k, n: wdo[k : k + n, layer * 256 : layer * 256 + 128]
             )
             gates[s] = jax.nn.sigmoid(total)
 
@@ -500,7 +504,7 @@
         ref = gm.at[layer, s, :, pl.ds(0, 896)]
         copy = remote(ref, e_sem.at[layer, s, 0], e_sem.at[layer, s, 1], place.partner())
         copy.wait_recv()
-        copy.wait_send()
+        waiting.append(copy)
         partial = dot(gm[layer, s], we[layer].reshape(1024, 512)).astype(BF16)
         for k in range(NX):
             tx[layer, s, k] = partial[:, k * 128 : k * 128 + 128]
@@ -519,7 +523,7 @@
         ref = rx.at[layer, s, pl.ds(0, 3)]
         copy = remote(ref, e_sem.at[layer, s, 2], e_sem.at[layer, s, 3], place.partner())
         copy.wait_recv()
-        copy.wait_send()
+        waiting.append(copy)
         branch = rx[layer, s, 0].astype(F32)
         for k in range(1, NX):
             branch = branch + rx[layer, s, k].astype(F32)
@@ -553,6 +557,8 @@
                     spread_mixed(layer, s, value)
             if kind < 2:
                 forward(layer, kind + 1)
+            for s in range(STREAMS):
+                gathers[layer, kind, s].drain()
             if kind == 0:
                 local[f"out{layer}"].start()
             for piece in relays.get((layer, kind), ()):
@@ -581,6 +587,8 @@
     theirs.wait_send()
     out_more[0, 0] = (jnp.max(counts[...]) > ROWS).astype(jnp.int32)
     weights.drain()
+    for copy in waiting:
+        copy.wait_send()
     for name in ("out0", "out1", "out_tokens"):
         local[name].wait()
 
@@ -623,6 +631,7 @@
             pltpu.VMEM((2, STREAMS, NZ, PART, 512), BF16),
             pltpu.VMEM((2, 2, STREAMS, NZ, half, 512), BF16),
             pltpu.VMEM((2, STREAMS, PART, 1024), BF16),
+            pltpu.VMEM((STREAMS, NZ, PART, 512), BF16),
             pltpu.VMEM((2, STREAMS, NX, PART, 128), BF16),
             pltpu.VMEM((2, STREAMS, NX, PART, 128), BF16),
             pltpu.VMEM((STREAMS, PART, 256), BF16),

time: 104 us -> 102 us (0.981)
  the two profiles are of different devices: /device:TPU:16 before, /device:TPU:32 now
where the time goes in v6:
time: 102 us; the launch traced here: 101 us
  Pallas kernels  97.3 us (95%)
  local copies, waits for them, and re-layouts  2.02 us (2%)
  between operations  1.34 us (1%)
    pallas_call x1, Pallas kernels, some(): return layers(number)(tokens, lengths, *rest, state)  97.3 us

profile of v6, /device:TPU:32, one launch (start us, length us, event | category | flops | bytes accessed | tf_op | source)
XLA Modules:
  0.0 100.9 jit_solution(14800361777924911856)
XLA Ops:
  0.6 0.0 copy-start.11
  0.6 0.0 copy-start.12
  0.7 0.0 copy-start.9
  0.7 0.0 copy-start.8
  0.7 0.0 copy-start.10
  0.7 0.6 copy-done.11
  1.3 0.0 copy-done.12
  1.3 0.0 copy-done.9
  1.4 0.0 copy-done.8
  1.4 0.0 copy-done.10
  1.4 0.0 copy-start
  1.4 0.0 copy-start.1
  1.4 0.0 copy-start.2
  1.4 0.0 copy-start.3
  1.4 0.0 copy-start.4
  1.4 0.0 copy-start.5
  1.4 0.0 copy-start.6
  1.4 0.0 copy-start.7
  1.4 97.3 %layers_0.1 = (bf16[256,128]{1,0:T(8,128)(2,1)S(1)}, f32[2,2,32,256]{3,2,1,0:T(8,128)S(1)}, s32[1,1]{1,0:T(1,128)}) custom-call(bf16[256,128]{1,0:T(8,128)(2,1)} %bitcast.19, s32[1,32]{1,0:T(1,128)S(1)} %bitcast.20, f32[2,4096]{1,0:T(2,128)} %gains_h.1, bf16[2,64,512]{2,1,0:T(8,128)(2,1)} %bitcast.10, bf16[2,512,128]{2,1,0:T(8,128)(2,1)} %opening_h.1, ...), custom_call_target="tpu_custom_call" | custom-call | tf_op jit(solution)/shard_map/layers_0/pallas_call | solution.py:681
  99.3 0.0 copy-done
  99.3 0.0 copy-done.1
  99.3 0.0 copy-done.2
  99.3 0.0 copy-done.3
  99.3 0.0 copy-done.4
  99.3 0.0 copy-done.5
  99.4 0.0 copy-done.6
  99.4 0.0 copy-done.7
  99.4 0.3 conditional.1
  99.6 0.6 copy.25
  100.3 0.7 copy.26
Async XLA Ops:
  0.6 0.7 copy-start.11
  0.6 0.7 copy-start.12
  0.7 0.7 copy-start.9
  0.7 0.7 copy-start.8
  0.7 0.7 copy-start.10
  1.4 97.9 %copy-start = (bf16[2,512,128]{2,1,0:T(8,128)(2,1)S(1)}, bf16[2,512,128]{2,1,0:T(8,128)(2,1)}, u32[]{:S(2)}) copy-start(bf16[2,512,128]{2,1,0:T(8,128)(2,1)} %opening_h.1) | copy-start | bytes 786436
  1.4 97.9 %copy-start.1 = (bf16[2,512,128]{2,1,0:T(8,128)(2,1)S(1)}, bf16[2,512,128]{2,1,0:T(8,128)(2,1)}, u32[]{:S(2)}) copy-start(bf16[2,512,128]{2,1,0:T(8,128)(2,1)} %leaving_h.1) | copy-start | bytes 786436
  1.4 97.9 %copy-start.2 = (bf16[2,512,64]{1,2,0:T(8,128)(2,1)S(1)}, bf16[2,512,64]{1,2,0:T(8,128)(2,1)}, u32[]{:S(2)}) copy-start(bf16[2,512,64]{1,2,0:T(8,128)(2,1)} %param.20) | copy-start | bytes 393220
  1.4 97.9 %copy-start.3 = (bf16[2,256,128]{2,1,0:T(8,128)(2,1)S(1)}, bf16[2,256,128]{2,1,0:T(8,128)(2,1)}, u32[]{:S(2)}) copy-start(bf16[2,256,128]{2,1,0:T(8,128)(2,1)} %merge_h.1) | copy-start | bytes 393220
  1.4 97.9 %copy-start.4 = (f32[2,2,4,64,16]{3,4,2,1,0:T(8,128)S(1)}, f32[2,2,4,64,16]{3,4,2,1,0:T(8,128)}, u32[]{:S(2)}) copy-start(f32[2,2,4,64,16]{3,4,2,1,0:T(8,128)} %param.28) | copy-start | bytes 196612
  1.4 97.9 %copy-start.5 = (f32[2,2,4,16,64]{4,3,2,1,0:T(8,128)S(1)}, f32[2,2,4,16,64]{4,3,2,1,0:T(8,128)}, u32[]{:S(2)}) copy-start(f32[2,2,4,16,64]{4,3,2,1,0:T(8,128)} %param.29) | copy-start | bytes 196612
  1.4 97.9 %copy-start.6 = (bf16[2,256,64]{1,2,0:T(8,128)(2,1)S(1)}, bf16[2,256,64]{1,2,0:T(8,128)(2,1)}, u32[]{:S(2)}) copy-start(bf16[2,256,64]{1,2,0:T(8,128)(2,1)} %param.22) | copy-start | bytes 196612
  1.4 97.9 %copy-start.7 = (f32[2,4096]{1,0:T(2,128)S(1)}, f32[2,4096]{1,0:T(2,128)}, u32[]{:S(2)}) copy-start(f32[2,4096]{1,0:T(2,128)} %gains_h.1) | copy-start | bytes 98308

commit v7 on v6

--- a/solution.py
+++ b/solution.py
@@ -13,6 +13,7 @@
 EPS = 1e-05
 NZ, NX, NY, NDP = 8, 4, 4, 8
 Z_ORDER, X_ORDER = (1, 7, 2, 6, 3, 5, 4), (2, 1, 3)
+Z_FAR, Z_MIXED = (4, 3, 5, 2, 6, 1, 7), (1, 7, 4, 3, 5, 2, 6)
 ROWS, STREAMS = 128, 2
 PART = ROWS // STREAMS
 LANES = 128
@@ -87,7 +88,7 @@
             remote(ref, self.send.at[1], self.recv.at[7], self.p.at_x(e)).start()
 
     def start(self):
-        for d in Z_ORDER:
+        for d in Z_MIXED:
             remote(self.block(0, 0), self.send.at[0], self.recv.at[d - 1], self.p.at_z(d)).start()
         self.along_x(self.block(0, 0))
 
@@ -496,7 +497,7 @@
     def spread_mixed(layer, s, value):
         lanes = pl.ds(pl.multiple_of(place.z * LANES, LANES), LANES)
         gm[layer, s, :, lanes] = value
-        for d in Z_ORDER:
+        for d in Z_FAR:
             ref = gm.at[layer, s, :, lanes]
             remote(ref, e_sem.at[layer, s, 0], e_sem.at[layer, s, 1], place.at_z(d)).start()
 

time: 102 us -> 100 us (0.980); the launches traced: 101 us -> 100 us
  no operation moved by 1% of the time
where the time goes in v7:
time: 100 us
  Pallas kernels  96.3 us (96%)
  local copies, waits for them, and re-layouts  2.02 us (2%)
  between operations  1.34 us (1%)
    pallas_call x1, Pallas kernels, some(): return layers(number)(tokens, lengths, *rest, state)  96.3 us
    unnamed x28, local copies, waits for them, and re-layouts  2.02 us

profile of v7, /device:TPU:32, one launch (start us, length us, event | category | flops | bytes accessed | tf_op | source)
XLA Modules:
  0.0 100.0 jit_solution(1514735208493972631)
XLA Ops:
  0.6 0.0 copy-start.11
  0.6 0.0 copy-start.12
  0.7 0.0 copy-start.9
  0.7 0.0 copy-start.8
  0.7 0.0 copy-start.10
  0.7 0.6 copy-done.11
  1.3 0.0 copy-done.12
  1.3 0.0 copy-done.9
  1.4 0.0 copy-done.8
  1.4 0.0 copy-done.10
  1.4 0.0 copy-start
  1.4 0.0 copy-start.1
  1.4 0.0 copy-start.2
  1.4 0.0 copy-start.3
  1.4 0.0 copy-start.4
  1.4 0.0 copy-start.5
  1.4 0.0 copy-start.6
  1.4 0.0 copy-start.7
  1.4 96.3 %layers_0.1 = (bf16[256,128]{1,0:T(8,128)(2,1)S(1)}, f32[2,2,32,256]{3,2,1,0:T(8,128)S(1)}, s32[1,1]{1,0:T(1,128)}) custom-call(bf16[256,128]{1,0:T(8,128)(2,1)} %bitcast.19, s32[1,32]{1,0:T(1,128)S(1)} %bitcast.20, f32[2,4096]{1,0:T(2,128)} %gains_h.1, bf16[2,64,512]{2,1,0:T(8,128)(2,1)} %bitcast.10, bf16[2,512,128]{2,1,0:T(8,128)(2,1)} %opening_h.1, ...), custom_call_target="tpu_custom_call" | custom-call | tf_op jit(solution)/shard_map/layers_0/pallas_call | solution.py:682
  98.3 0.0 copy-done
  98.3 0.0 copy-done.1
  98.3 0.0 copy-done.2
  98.4 0.0 copy-done.3
  98.4 0.0 copy-done.4
  98.4 0.0 copy-done.5
  98.4 0.0 copy-done.6
  98.4 0.0 copy-done.7
  98.4 0.3 conditional.1
  98.7 0.6 copy.25
  99.3 0.7 copy.26
Async XLA Ops:
  0.6 0.7 copy-start.11
  0.6 0.7 copy-start.12
  0.7 0.7 copy-start.9
  0.7 0.7 copy-start.8
  0.7 0.7 copy-start.10
  1.4 96.9 %copy-start = (bf16[2,512,128]{2,1,0:T(8,128)(2,1)S(1)}, bf16[2,512,128]{2,1,0:T(8,128)(2,1)}, u32[]{:S(2)}) copy-start(bf16[2,512,128]{2,1,0:T(8,128)(2,1)} %opening_h.1) | copy-start | bytes 786436
  1.4 97.0 %copy-start.1 = (bf16[2,512,128]{2,1,0:T(8,128)(2,1)S(1)}, bf16[2,512,128]{2,1,0:T(8,128)(2,1)}, u32[]{:S(2)}) copy-start(bf16[2,512,128]{2,1,0:T(8,128)(2,1)} %leaving_h.1) | copy-start | bytes 786436
  1.4 97.0 %copy-start.2 = (bf16[2,512,64]{1,2,0:T(8,128)(2,1)S(1)}, bf16[2,512,64]{1,2,0:T(8,128)(2,1)}, u32[]{:S(2)}) copy-start(bf16[2,512,64]{1,2,0:T(8,128)(2,1)} %param.20) | copy-start | bytes 393220
  1.4 97.0 %copy-start.3 = (bf16[2,256,128]{2,1,0:T(8,128)(2,1)S(1)}, bf16[2,256,128]{2,1,0:T(8,128)(2,1)}, u32[]{:S(2)}) copy-start(bf16[2,256,128]{2,1,0:T(8,128)(2,1)} %merge_h.1) | copy-start | bytes 393220
  1.4 97.0 %copy-start.4 = (f32[2,2,4,64,16]{3,4,2,1,0:T(8,128)S(1)}, f32[2,2,4,64,16]{3,4,2,1,0:T(8,128)}, u32[]{:S(2)}) copy-start(f32[2,2,4,64,16]{3,4,2,1,0:T(8,128)} %param.28) | copy-start | bytes 196612
  1.4 97.0 %copy-start.5 = (f32[2,2,4,16,64]{4,3,2,1,0:T(8,128)S(1)}, f32[2,2,4,16,64]{4,3,2,1,0:T(8,128)}, u32[]{:S(2)}) copy-start(f32[2,2,4,16,64]{4,3,2,1,0:T(8,128)} %param.29) | copy-start | bytes 196612
  1.4 97.0 %copy-start.6 = (bf16[2,256,64]{1,2,0:T(8,128)(2,1)S(1)}, bf16[2,256,64]{1,2,0:T(8,128)(2,1)}, u32[]{:S(2)}) copy-start(bf16[2,256,64]{1,2,0:T(8,128)(2,1)} %param.22) | copy-start | bytes 196612
  1.4 97.0 %copy-start.7 = (f32[2,4096]{1,0:T(2,128)S(1)}, f32[2,4096]{1,0:T(2,128)}, u32[]{:S(2)}) copy-start(f32[2,4096]{1,0:T(2,128)} %gains_h.1) | copy-start | bytes 98308
